TPU v7x, 32 devices: a whole 2x2x4 slice. The times are simulated.
32 devices in a mesh: st: 16 (over z, y, x), tp: 2 (over core).
Axes of the slice: x: 2, y: 2, z: 4, core: 2. Of those that a mesh axis runs over, the one named last changes fastest.
Arguments:
- hidden: bfloat16 [16384, 2048], P('st'), may hold values from -6 to 6
- norm_gain: float32 [2048], replicated, may hold values from 0.1 to 1.9
- store: bfloat16 [384, 64, 2048], P('st'), may hold values from -6 to 6
- store_gain: float32 [2048], replicated, may hold values from 0.1 to 1.9
- passage_ids: int32 [128, 4], P('st'), may hold values from 0 to 383, as said below
- w_pool: bfloat16 [2048, 1024], P(None, 'tp'), may hold values from -0.125 to 0.125
- pool_mix: bfloat16 [4, 256, 256], P('tp'), may hold values from -0.375 to 0.375
- w_branch: bfloat16 [1024, 2048], P('tp'), may hold values from -0.1875 to 0.1875
- w_query: bfloat16 [2048, 512], P(None, 'tp'), may hold values from -0.125 to 0.125
- w_key: bfloat16 [2048, 512], P(None, 'tp'), may hold values from -0.125 to 0.125
- w_value: bfloat16 [2048, 512], P(None, 'tp'), may hold values from -0.125 to 0.125
- sharpness: float32 [4], P('tp'), may hold values from 1 to 90
- w_out: bfloat16 [512, 2048], P('tp'), may hold values from -0.25 to 0.25
- w_gate: bfloat16 [2048, 2048], P(None, 'tp'), may hold values from -0.125 to 0.125
Outputs:
- mixed: bfloat16 [16384, 2048], P('st', 'tp')
Inputs may be any that keep to these rules, and one draw needn't show every extreme that they name: `passage_ids`: passage p lies on index p // 24 of st. The ids of one sequence's blocks (aligned rows of 32 ids) name passages of at most 4 reads on any one holder, counted with repeats, and some sequence reaches 4 at some holder in every draw.
All inputs are finite; a program needn't handle non-finite values.
Results may differ from a plain program's by a relative error of at most 0.0095.
The roundings to bfloat16 on the way count: a program that leaves them out, or rounds other values in their place, can miss the bound.
Values may be sent and summed in bfloat16 or wider, within the bound.
A program may use at most 128 MiB of HBM per device.

v0:
```python
import functools
import math

import jax
import jax.numpy as jnp
from jax import lax
from jax.experimental import pallas as pl
from jax.experimental.pallas import tpu as pltpu
from jax.sharding import PartitionSpec as P

GROUPS = 4
ATTEND_BLOCKS = 8
MESH = pl.DeviceIdType.MESH


def rms_norm(values, gain):
    wide = values.astype(jnp.float32)
    scale = lax.rsqrt(jnp.mean(wide * wide, axis=-1, keepdims=True) + 1e-05)
    return wide * scale * gain


def pool_branch(normed, w_pool, pool_mix):
    tokens = normed.shape[0]
    local_groups = pool_mix.shape[0]
    group_dim = pool_mix.shape[1]
    pool_in = jnp.dot(normed, w_pool, preferred_element_type=jnp.float32).astype(jnp.bfloat16)
    grouped = pool_in.astype(jnp.float32).reshape(tokens, local_groups, group_dim)
    group_index = lax.axis_index("tp") * local_groups + jnp.arange(local_groups, dtype=jnp.int32)
    window = jnp.power(2, group_index + 1)
    total = jnp.zeros_like(grouped)
    for shift in range(2**GROUPS):
        shifted = jnp.pad(grouped, ((shift, 0), (0, 0), (0, 0)))[:tokens]
        total = total + jnp.where(shift < window, 1.0, 0.0)[None, :, None] * shifted
    position = jnp.arange(tokens, dtype=jnp.int32)[:, None]
    count = jnp.minimum(position + 1, window[None, :]).astype(jnp.float32)
    pooled = (total / count[:, :, None] - grouped).astype(jnp.bfloat16)
    pool_out = jnp.einsum("tgc,gcd->tgd", pooled, pool_mix, preferred_element_type=jnp.float32)
    return pool_out.astype(jnp.bfloat16).reshape(tokens, local_groups * group_dim)


def half_terms(own, other, weight_own, weight_other):
    terms = [
        jnp.dot(a, w, preferred_element_type=jnp.float32).astype(jnp.bfloat16).astype(jnp.float32)
        for a, w in ((own, weight_own), (other, weight_other))
    ]
    return terms[0] + terms[1]


def swap(array):
    return lax.ppermute(array, "tp", [(0, 1), (1, 0)])


def columns_of(weight, part):
    half = weight.shape[1] // 2
    return lax.dynamic_slice_in_dim(weight, part * half, half, axis=1)


def attention_kernel(heads, group, slots_ref, scale_ref, q_ref, *refs):
    parts, out_ref = refs[:-1], refs[-1]
    width = q_ref.shape[1]
    head_dim = width // heads
    block_len = q_ref.shape[0] // group
    per_block = len(parts) // group
    for b, h in [(b, h) for b in range(group) for h in range(heads)]:
        rows = slice(b * block_len, (b + 1) * block_len)
        kv = jnp.concatenate([r[0] for r in parts[b * per_block : (b + 1) * per_block]], axis=0)
        cut = slice(h * head_dim, (h + 1) * head_dim)
        scores = lax.dot_general(
            q_ref[rows, cut], kv[:, cut], (((1,), (1,)), ((), ())), preferred_element_type=jnp.float32
        )
        scores = scores * scale_ref[h]
        top = jnp.exp(scores - jnp.max(scores, axis=-1, keepdims=True))
        weights = (top * (1.0 / jnp.sum(top, axis=-1, keepdims=True))).astype(jnp.bfloat16)
        out_ref[rows, cut] = jnp.dot(
            weights, kv[:, width + h * head_dim : width + (h + 1) * head_dim],
            preferred_element_type=jnp.float32,
        ).astype(jnp.bfloat16)


def attend(query, kv, block_slot, scale):
    blocks_dev, per_block = block_slot.shape
    tokens, width = query.shape
    block_len = tokens // blocks_dev
    length, both = kv.shape[1:]
    heads = scale.shape[0]
    group = math.gcd(blocks_dev, ATTEND_BLOCKS)
    taken = group * per_block

    def part(j):
        return pl.BlockSpec((1, length, both), lambda b, slots: (slots[b * taken + j], 0, 0))

    return pl.pallas_call(
        functools.partial(attention_kernel, heads, group),
        out_shape=jax.ShapeDtypeStruct((tokens, width), jnp.bfloat16),
        grid_spec=pltpu.PrefetchScalarGridSpec(
            num_scalar_prefetch=1,
            grid=(blocks_dev // group,),
            in_specs=[
                pl.BlockSpec(memory_space=pltpu.SMEM),
                pl.BlockSpec((group * block_len, width), lambda b, slots: (b, 0)),
            ] + [part(j) for j in range(taken)],
            out_specs=pl.BlockSpec((group * block_len, width), lambda b, slots: (b, 0)),
        ),
        cost_estimate=pl.CostEstimate(
            flops=4 * tokens * per_block * length * width, bytes_accessed=4 * 2**20, transcendentals=0
        ),
    )(block_slot.reshape(-1), scale, query, *([kv] * taken))


def body(
    hidden,
    norm_gain,
    store,
    store_gain,
    passage_ids,
    w_pool,
    pool_mix,
    w_branch,
    w_query,
    w_key,
    w_value,
    sharpness,
    w_out,
    w_gate,
):
    holders = lax.axis_size("st")
    core = lax.axis_index("tp")
    flat_ids = passage_ids.reshape(-1)
    reads = flat_ids.shape[0]
    pass_dev, length, width = store.shape
    owner = lax.div(flat_ids, pass_dev)
    local = flat_ids - owner * pass_dev
    order = jnp.arange(reads, dtype=jnp.int32)
    earlier = (owner[None, :] == owner[:, None]) & (order[None, :] < order[:, None])
    rank = jnp.sum(earlier.astype(jnp.int32), axis=1)
    most = max(1, 2 * reads // holders)
    wanted = owner * most + rank
    hits = wanted[None, :] == jnp.arange(holders * most, dtype=jnp.int32)[:, None]
    request = jnp.sum(jnp.where(hits, local[None, :], 0), axis=1).reshape(holders, most)
    incoming = lax.all_to_all(request, "st", split_axis=0, concat_axis=0, tiled=True)

    passage_normed = rms_norm(store, store_gain).astype(jnp.bfloat16).reshape(pass_dev * length, width)
    w_kv = jnp.concatenate([w_key, w_value], axis=1)
    own_kv = jnp.dot(passage_normed, w_kv, preferred_element_type=jnp.float32).astype(jnp.bfloat16)
    own_kv = own_kv.reshape(pass_dev, length, -1)
    packed = own_kv[incoming.reshape(-1)]
    packed, hidden, w_out, w_branch = lax.optimization_barrier((packed, hidden, w_out, w_branch))
    kv = lax.all_to_all(packed, "st", split_axis=0, concat_axis=0, tiled=True)
    slot = wanted

    w_out_other = swap(columns_of(w_out, 1 - core))
    w_branch_other = swap(columns_of(w_branch, 1 - core))
    normed = rms_norm(hidden, norm_gain).astype(jnp.bfloat16)
    pool_out = pool_branch(normed, w_pool, pool_mix)
    branch_pool = half_terms(pool_out, swap(pool_out), columns_of(w_branch, core), w_branch_other)
    gate = jax.nn.sigmoid(jnp.dot(normed, w_gate, preferred_element_type=jnp.float32))
    query = jnp.dot(normed, w_query, preferred_element_type=jnp.float32).astype(jnp.bfloat16)

    head_dim = query.shape[1] // sharpness.shape[0]
    read = attend(query, kv, slot.reshape(passage_ids.shape), sharpness / math.sqrt(head_dim))
    branch_read = half_terms(read, swap(read), columns_of(w_out, core), w_out_other)
    return (branch_pool + gate * branch_read).astype(jnp.bfloat16)


def solution(mesh):
    placed = (
        P("st", None),
        P(),
        P("st", None, None),
        P(),
        P("st", None),
        P(None, "tp"),
        P("tp", None, None),
        P("tp", None),
        P(None, "tp"),
        P(None, "tp"),
        P(None, "tp"),
        P("tp"),
        P("tp", None),
        P(None, "tp"),
    )
    return jax.shard_map(body, mesh=mesh, in_specs=placed, out_specs=P("st", "tp"), check_vma=False)
```

profile of v0, /device:TPU:13, one launch (start us, length us, event | category | flops | bytes accessed | tf_op | source)
XLA Modules:
  0.0 139.7 jit_solution(13067067701625103407)
XLA Ops:
  0.0 0.9 copy.73
  1.3 0.7 all_to_all.9
  2.0 6.6 %all-to-all-start = ((s32[16,1,4]{2,1,0:T(1,128)}), s32[16,1,4]{2,1,0:T(1,128)S(1)}, u32[]{:S(2)}, u32[]{:S(2)}) async-start(s32[16,1,4]{2,1,0:T(1,128)} %bitcast.2), calls=%async_computation | async-start | bytes 16384 | tf_op jit(solution)/shard_map/all_to_all | solution.py:140
  8.6 4.2 %fusion = f32[24,64]{1,0:T(8,128)S(1)} fusion(bf16[24,64,2048]{2,1,0:T(8,128)(2,1)} %param.16), kind=kLoop, calls=%fused_computation.3 | loop fusion | flops 9435648 | bytes 6297600 | tf_op jit(solution)/shard_map/reduce_sum | solution.py:18
  13.2 1.5 %fusion.2 = bf16[24,64,2048]{2,1,0:T(8,128)(2,1)S(1)} fusion(bf16[24,64,2048]{2,1,0:T(8,128)(2,1)S(1)} %copy-done.1, f32[2048]{0:T(1024)S(1)} %copy-done.7, f32[24,64]{1,0:T(8,128)S(1)} %add_rsqrt_fusion), kind=kLoop, calls=%fused_computation.5 | loop fusion | flops 12582912 | bytes 12597248 | tf_op jit(solution)/shard_map/convert_element_type | solution.py:142
  14.7 4.8 %convolution_convert_fusion = bf16[1536,512]{1,0:T(8,128)(2,1)} fusion(bf16[1536,2048]{1,0:T(8,128)(2,1)S(1)} %bitcast.22, bf16[2048,256]{1,0:T(8,128)(2,1)S(1)} %copy-done.10, bf16[2048,256]{1,0:T(8,128)(2,1)S(1)} %copy-done.11), kind=kOutput, calls=%fused_computation.12 | convolution fusion | flops 3226206208 | bytes 9961472 | tf_op jit(solution)/shard_map/dot_general | solution.py:144
  20.7 4.2 %gather_fusion = bf16[64,64,512]{2,1,0:T(8,128)(2,1)} fusion(bf16[24,64,512]{2,1,0:T(8,128)(2,1)} %bitcast.21, s32[1024]{0:T(1024)S(1)} %pad_clamp_fusion), kind=kCustom, calls=%fused_computation | custom fusion | bytes 8388864 | tf_op jit(solution)/shard_map/gather | solution.py:146
  24.9 6.5 %all-to-all-start.1 = ((bf16[64,64,512]{2,1,0:T(8,128)(2,1)}), bf16[64,64,512]{2,1,0:T(8,128)(2,1)}, u32[]{:S(2)}, u32[]{:S(2)}) async-start(bf16[64,64,512]{2,1,0:T(8,128)(2,1)} %gather_fusion), calls=%async_computation.1 | async-start | bytes 8388608 | tf_op jit(solution)/shard_map/all_to_all | solution.py:148
  32.3 0.9 constant_dynamic-slice_fusion
  33.1 1.8 %collective-permute-start.3 = (bf16[256,1024]{1,0:T(8,128)(2,1)}, bf16[256,1024]{1,0:T(8,128)(2,1)}, u32[]{:S(2)}, u32[]{:S(2)}) collective-permute-start(bf16[256,1024]{1,0:T(8,128)(2,1)} %constant_dynamic-slice_fusion), channel_id=1, source_target_pairs={{0,1},{1,0},{2,3},{3,2},{4,5},{5,4},{6,7},{7,6},{8,9},{9,8},{10,11... | collective-permute-start | bytes 1572872 | tf_op jit(solution)/shard_map/ppermute | solution.py:50
  34.9 3.1 %fusion.3 = f32[1024]{0:T(1024)S(1)} fusion(bf16[1024,2048]{1,0:T(8,128)(2,1)} %param.14), kind=kLoop, calls=%fused_computation.8 | loop fusion | flops 6290432 | bytes 4198400 | tf_op jit(solution)/shard_map/reduce_sum | solution.py:18
  38.0 4.2 %convolution_convert_fusion.2 = bf16[1024,512]{0,1:T(8,128)(2,1)S(1)} fusion(bf16[2048,512]{1,0:T(8,128)(2,1)} %param.19, bf16[1024,2048]{1,0:T(8,128)(2,1)S(1)} %copy-done.2, f32[2048]{0:T(1024)S(1)} %copy-done.14, f32[1024]{0:T(1024)S(1)} %add_rsqrt_fusion.1), kind=kOutput, calls=%fused_computation.63 | convolution fusion | flops 2156396544 | bytes 7352320 | tf_op jit(solution)/shard_map/dot_general | solution.py:26
  42.2 1.6 %copy.75 = f32[1024,2,256]{2,0,1:T(8,128)} copy(bf16[1024,2,256]{0,2,1:T(8,128)(2,1)S(1)} %bitcast.23) | data formatting | bytes 3145728 | tf_op jit(solution)/shard_map/reshape | solution.py:27
  43.8 18.1 %convolution_convert_fusion.1 = bf16[2,1024,256]{1,2,0:T(8,128)(2,1)} fusion(bf16[2,256,256]{2,1,0:T(8,128)(2,1)S(1)} %copy-done.13, f32[1024,2,256]{2,0,1:T(8,128)} %copy.75, f32[1024,2]{0,1:T(2,128)S(1)} %minimum_convert_fusion, f32[2]{0:T(128)S(1)} %get-tuple-element.15, f32[2]{0:T(128)S(1)} %get-tuple-element.16, f32[2]{0:T(128)S(1)} %get-tuple-element.17, ...), kind=kOutput, calls=%fused_computation.62 | convolution fusion | flops 286785536 | bytes 3416192 | tf_op jit(solution)/shard_map/tgc,gcd->tgd/dot_general | solution.py:37
  62.7 4.0 %fusion.39 = bf16[1024,1024]{1,0:T(8,128)(2,1)} fusion(bf16[1024,512]{0,1:T(8,128)(2,1)} %bitcast.7, bf16[512,2048]{1,0:T(8,128)(2,1)S(1)} %copy-done, s32[]{:T(128)S(6)} %select_n.499), kind=kOutput, calls=%fused_computation.65 | convolution fusion | flops 1073741824 | bytes 4194308 | tf_op jit(solution)/shard_map/dot_general | solution.py:43
  66.7 2.1 %convolution_convert_fusion.3.q_ref = bf16[1024,256]{1,0:T(8,128)(2,1)} fusion(bf16[2048,256]{1,0:T(8,128)(2,1)S(1)} %copy-done.12, bf16[1024,2048]{1,0:T(8,128)(2,1)S(1)} %copy-done.3, f32[2048]{0:T(1024)S(1)} %copy-done.14, f32[1024]{0:T(1024)S(1)} %add_rsqrt_fusion.1), kind=kOutput, calls=%fused_computation.64 | convolution fusion | flops 1082392576 | bytes 5779456 | tf_op jit(solution)/shard_map/dot_general | solution.py:157
  68.9 6.3 %fusion.50 = f32[1024,1024]{1,0:T(8,128)} fusion(bf16[2048,1024]{1,0:T(8,128)(2,1)S(1)} %copy-done.9, bf16[1024,2048]{1,0:T(8,128)(2,1)S(1)} %copy-done.3, f32[2048]{0:T(1024)S(1)} %copy-done.14, f32[1024]{0:T(1024)S(1)} %add_rsqrt_fusion.1), kind=kOutput, calls=%fused_computation.113 | convolution fusion | flops 4303355904 | bytes 12595200 | tf_op jit(solution)/shard_map/dot_general | solution.py:156
  75.1 49.6 %all-to-all-done.1.refs_0_.refs_1_.refs_2_.refs_3_.refs_4_.refs_5_.refs_6_.refs_7_.refs_8_.refs_9_.refs_10_.refs_11_.refs_12_.refs_13_.refs_14_.refs_15_.refs_16_.refs_17_.refs_18_.refs_19_.refs_20_.refs_21_.refs_22_.refs_23_.refs_24_.refs_25_.refs_26_.refs_27_.refs_28_.refs_29_.refs_30_.refs_31_ = bf16[64,64,512]{2,1,0:T(8,128)(2,1)} async-done(((bf16[64,64,512]{2,1,0:T(8,128)(2,1)}), ...) | async-done | bytes 4194336 | tf_op jit(solution)/shard_map/all_to_all | solution.py:148
  124.7 4.8 %shard_map.136 = bf16[1024,256]{1,0:T(8,128)(2,1)} custom-call(s32[32]{0:T(128)} %copy-done.8, f32[2]{0:T(128)} %broadcast_multiply_fusion.scale_ref, bf16[1024,256]{1,0:T(8,128)(2,1)} %convolution_convert_fusion.3.q_ref, ...), custom_call_target="tpu_custom_call" | custom-call | flops 268435456 | bytes 4194304 | tf_op jit(solution)/shard_map/pallas_call | solution.py:92
  129.6 1.5 %collective-permute-start.2 = (bf16[1024,256]{1,0:T(8,128)(2,1)}, bf16[1024,256]{1,0:T(8,128)(2,1)S(1)}, u32[]{:S(2)}, u32[]{:S(2)}) collective-permute-start(bf16[1024,256]{1,0:T(8,128)(2,1)} %shard_map.136), channel_id=1, source_target_pairs={{0,1},{1,0},{2,3},{3,2},{4,5},{5,4},{6,7},{7,6},{8,9},{9,8},{10,11... | collective-permute-start | bytes 1572872 | tf_op jit(solution)/shard_map/ppermute | solution.py:50
  131.0 3.0 %fusion.53 = bf16[1024,1024]{1,0:T(8,128)(2,1)S(1)} fusion(bf16[1024,512]{0,1:T(8,128)(2,1)} %collective-permute-done, bf16[512,1024]{1,0:T(8,128)(2,1)} %collective-permute-done.1), kind=kOutput, calls=%fused_computation.114 | convolution fusion | flops 1073741824 | bytes 4194304 | tf_op jit(solution)/shard_map/dot_general | solution.py:43
  134.1 0.7 fusion.41
  134.8 0.8 copy-done.16
  135.7 4.1 %add_convert_fusion = bf16[1024,1024]{1,0:T(8,128)(2,1)} fusion(f32[1024,1024]{1,0:T(8,128)S(1)} %copy-done.17, bf16[1024,1024]{1,0:T(8,128)(2,1)S(1)} %fusion.41, bf16[1024,1024]{1,0:T(8,128)(2,1)S(1)} %fusion.53, bf16[1024,1024]{1,0:T(8,128)(2,1)S(1)} %copy-done.16, bf16[1024,256]{1,0:T(8,128)(2,1)S(1)} %collective-permute-done.2, ...), kind=kOutput, calls=%fused_computation.11 | convolution fusion | flops 550502400 | bytes 13631488 | tf_op jit(solution)/shard_map/dot_general | solution.py:43
  (67 shorter events, 3.6 us)
Async XLA Ops:
  0.0 62.3 %copy-start = (bf16[512,2048]{1,0:T(8,128)(2,1)S(1)}, bf16[512,2048]{1,0:T(8,128)(2,1)}, u32[]{:S(2)}) copy-start(bf16[512,2048]{1,0:T(8,128)(2,1)} %param.21) | copy-start | bytes 6291460
  1.2 11.7 %copy-start.8 = (s32[32]{0:T(128)}, s32[32]{0:T(128)S(1)}, u32[]{:S(2)}) copy-start(s32[32]{0:T(128)S(1)} %multiply_add_fusion.slots_ref) | copy-start | bytes 388
  2.0 17.5 %all-to-all-start = ((s32[16,1,4]{2,1,0:T(1,128)}), s32[16,1,4]{2,1,0:T(1,128)S(1)}, u32[]{:S(2)}, u32[]{:S(2)}) async-start(s32[16,1,4]{2,1,0:T(1,128)} %bitcast.2), calls=%async_computation | async-start | bytes 16384 | tf_op jit(solution)/shard_map/all_to_all | solution.py:140
  8.6 4.6 %copy-start.1 = (bf16[24,64,2048]{2,1,0:T(8,128)(2,1)S(1)}, bf16[24,64,2048]{2,1,0:T(8,128)(2,1)}, u32[]{:S(2)}) copy-start(bf16[24,64,2048]{2,1,0:T(8,128)(2,1)} %param.16) | copy-start | bytes 18874372
  8.6 4.6 %copy-start.7 = (f32[2048]{0:T(1024)S(1)}, f32[2048]{0:T(1024)}, u32[]{:S(2)}) copy-start(f32[2048]{0:T(1024)} %param.17) | copy-start | bytes 24580
  13.2 1.5 %copy-start.10 = (bf16[2048,256]{1,0:T(8,128)(2,1)S(1)}, bf16[2048,256]{1,0:T(8,128)(2,1)}, u32[]{:S(2)}) copy-start(bf16[2048,256]{1,0:T(8,128)(2,1)} %param.24) | copy-start | bytes 3145732
  13.2 1.5 %copy-start.11 = (bf16[2048,256]{1,0:T(8,128)(2,1)S(1)}, bf16[2048,256]{1,0:T(8,128)(2,1)}, u32[]{:S(2)}) copy-start(bf16[2048,256]{1,0:T(8,128)(2,1)} %param.23) | copy-start | bytes 3145732
  24.9 6.7 %copy-start.15 = (f32[2]{0:T(128)S(1)}, f32[2]{0:T(128)}, u32[]{:S(2)}) copy-start(f32[2]{0:T(128)} %param.25) | copy-start | bytes 28
  24.9 7.3 %copy-start.5 = (bf16[256,2048]{1,0:T(8,128)(2,1)S(1)}, bf16[256,2048]{1,0:T(8,128)(2,1)}, u32[]{:S(2)}) copy-start(bf16[256,2048]{1,0:T(8,128)(2,1)} %param.26) | copy-start | bytes 3145732
  24.9 99.8 %all-to-all-start.1 = ((bf16[64,64,512]{2,1,0:T(8,128)(2,1)}), bf16[64,64,512]{2,1,0:T(8,128)(2,1)}, u32[]{:S(2)}, u32[]{:S(2)}) async-start(bf16[64,64,512]{2,1,0:T(8,128)(2,1)} %gather_fusion), calls=%async_computation.1 | async-start | bytes 8388608 | tf_op jit(solution)/shard_map/all_to_all | solution.py:148
  33.1 4.9 %copy-start.2 = (bf16[1024,2048]{1,0:T(8,128)(2,1)S(1)}, bf16[1024,2048]{1,0:T(8,128)(2,1)}, u32[]{:S(2)}) copy-start(bf16[1024,2048]{1,0:T(8,128)(2,1)} %param.14) | copy-start | bytes 12582916
  33.1 4.9 %copy-start.14 = (f32[2048]{0:T(1024)S(1)}, f32[2048]{0:T(1024)}, u32[]{:S(2)}) copy-start(f32[2048]{0:T(1024)} %param.15) | copy-start | bytes 24580
  33.1 101.7 %collective-permute-start.3 = (bf16[256,1024]{1,0:T(8,128)(2,1)}, bf16[256,1024]{1,0:T(8,128)(2,1)}, u32[]{:S(2)}, u32[]{:S(2)}) collective-permute-start(bf16[256,1024]{1,0:T(8,128)(2,1)} %constant_dynamic-slice_fusion), channel_id=1, source_target_pairs={{0,1},{1,0},{2,3},{3,2},{4,5},{5,4},{6,7},{7,6},{8,9},{9,8},{10,11... | collective-permute-start | bytes 1572872 | tf_op jit(solution)/shard_map/ppermute | solution.py:50
  42.2 1.6 %copy-start.13 = (bf16[2,256,256]{2,1,0:T(8,128)(2,1)S(1)}, bf16[2,256,256]{2,1,0:T(8,128)(2,1)}, u32[]{:S(2)}) copy-start(bf16[2,256,256]{2,1,0:T(8,128)(2,1)} %param.20) | copy-start | bytes 786436
  61.9 69.1 %collective-permute-start = (bf16[1024,512]{0,1:T(8,128)(2,1)}, bf16[1024,512]{0,1:T(8,128)(2,1)}, u32[]{:S(2)}, u32[]{:S(2)}) collective-permute-start(bf16[1024,512]{0,1:T(8,128)(2,1)} %bitcast.7), channel_id=1, source_target_pairs={{0,1},{1,0},{2,3},{3,2},{4,5},{5,4},{6,7},{7,6},{8,9},{9,8},{10,11... | collective-permute-start | bytes 3145736 | tf_op jit(solution)/shard_map/ppermute | solution.py:50
  62.4 4.3 %copy-start.3 = (bf16[1024,2048]{1,0:T(8,128)(2,1)S(1)}, bf16[1024,2048]{1,0:T(8,128)(2,1)}, u32[]{:S(2)}) copy-start(bf16[1024,2048]{1,0:T(8,128)(2,1)} %param.14) | copy-start | bytes 12582916
  62.4 4.2 %copy-start.12 = (bf16[2048,256]{1,0:T(8,128)(2,1)S(1)}, bf16[2048,256]{1,0:T(8,128)(2,1)}, u32[]{:S(2)}) copy-start(bf16[2048,256]{1,0:T(8,128)(2,1)} %param.22) | copy-start | bytes 3145732
  62.4 68.6 %collective-permute-start.1 = (bf16[512,1024]{1,0:T(8,128)(2,1)S(1)}, bf16[512,1024]{1,0:T(8,128)(2,1)}, u32[]{:S(2)}, u32[]{:S(2)}) collective-permute-start(bf16[512,1024]{1,0:T(8,128)(2,1)S(1)} %constant_dynamic-slice_fusion.1), channel_id=1, source_target_pairs={{0,1},{1,0},{2,3},{3,2},{4,5},{5,4},{6,7},{7,6},{8,9},{9,8},{10,11... | collective-permute-start | bytes 3145736 | tf_op jit(solution)/shard_map/ppermute | solution.py:50
  66.7 2.2 %copy-start.9 = (bf16[2048,1024]{1,0:T(8,128)(2,1)S(1)}, bf16[2048,1024]{1,0:T(8,128)(2,1)}, u32[]{:S(2)}) copy-start(bf16[2048,1024]{1,0:T(8,128)(2,1)} %param.27) | copy-start | bytes 12582916
  129.5 4.5 %copy-start.4 = (bf16[1024,256]{1,0:T(8,128)(2,1)S(1)}, bf16[1024,256]{1,0:T(8,128)(2,1)}, u32[]{:S(2)}) copy-start(bf16[1024,256]{1,0:T(8,128)(2,1)} %shard_map.136) | copy-start | bytes 1572868
  129.6 4.5 %copy-start.6 = (bf16[256,2048]{1,0:T(8,128)(2,1)S(1)}, bf16[256,2048]{1,0:T(8,128)(2,1)}, u32[]{:S(2)}) copy-start(bf16[256,2048]{1,0:T(8,128)(2,1)} %param.26) | copy-start | bytes 3145732
  129.6 5.2 %collective-permute-start.2 = (bf16[1024,256]{1,0:T(8,128)(2,1)}, bf16[1024,256]{1,0:T(8,128)(2,1)S(1)}, u32[]{:S(2)}, u32[]{:S(2)}) collective-permute-start(bf16[1024,256]{1,0:T(8,128)(2,1)} %shard_map.136), channel_id=1, source_target_pairs={{0,1},{1,0},{2,3},{3,2},{4,5},{5,4},{6,7},{7,6},{8,9},{9,8},{10,11... | collective-permute-start | bytes 1572872 | tf_op jit(solution)/shard_map/ppermute | solution.py:50
  131.0 3.8 %copy-start.17 = (f32[1024,1024]{1,0:T(8,128)S(1)}, f32[1024,1024]{1,0:T(8,128)}, u32[]{:S(2)}) copy-start(f32[1024,1024]{1,0:T(8,128)} %fusion.50) | copy-start | bytes 12582916
  134.1 1.6 %copy-start.16 = (bf16[1024,1024]{1,0:T(8,128)(2,1)S(1)}, bf16[1024,1024]{1,0:T(8,128)(2,1)}, u32[]{:S(2)}) copy-start(bf16[1024,1024]{1,0:T(8,128)(2,1)} %fusion.39) | copy-start | bytes 6291460
where the time goes:
time: 140 us
  waiting for transfers between devices  49.6 us (35%)
  matrix products  47.2 us (34%)
  starting transfers between devices  17 us (12%)
  other arithmetic  10.5 us (8%)
  local copies, waits for them, and re-layouts  10.3 us (7%)
  Pallas kernels  4.83 us (3%)
    all_to_all x1, waiting for transfers between devices, body(): kv = lax.all_to_all(packed, 'st', split_axis=0, concat_axis=0, tiled=True)  49.6 us
    dot_general x1, matrix products, pool_branch(): jnp.einsum('tgc,gcd->tgd', pooled, pool_mix, preferred_element_type=jnp.f...  18.1 us
    dot_general x4, matrix products, half_terms(): jnp.dot(a, w, preferred_element_type=jnp.float32).astype(jnp.bfloat16)  11.8 us
    reduce_sum x2, other arithmetic, rms_norm(): scale = lax.rsqrt(jnp.mean(wide * wide, axis=-1, keepdims=True) + 1e-05)  7.3 us
    all_to_all x1, starting transfers between devices, body(): lax.all_to_all(request, 'st', split_axis=0, concat_axis=0, tiled=True)  6.61 us
    all_to_all x1, starting transfers between devices, body(): kv = lax.all_to_all(packed, 'st', split_axis=0, concat_axis=0, tiled=True)  6.49 us
    dot_general x1, matrix products, body(): jnp.dot(normed, w_gate, preferred_element_type=jnp.float32)  6.27 us
    pallas_call x1, Pallas kernels, attend(): pl.pallas_call(functools.partial(attention_kernel, heads, group), out_sha...  4.83 us
  transfers between devices with their start and end apart: 6, of which 1 were waited for; matrix products, arithmetic and copies ran while one was open for 40% of the time, Pallas kernels for 3%

commit v1 on v0

v1 whole, which is shorter than its diff:
```python
import functools
import math

import jax
import jax.numpy as jnp
from jax import lax
from jax.experimental import pallas as pl
from jax.experimental.pallas import tpu as pltpu
from jax.sharding import PartitionSpec as P

MESH = pl.DeviceIdType.MESH
F32 = jnp.float32
BF16 = jnp.bfloat16
ANY = pl.BlockSpec(memory_space=pl.ANY)
VMEM = pl.BlockSpec(memory_space=pltpu.VMEM)
SMEM = pl.BlockSpec(memory_space=pltpu.SMEM)
LIMIT = 66_000_000


def planes_of(mesh):
    heights = {getattr(d, "coords", (0, 0, 0))[2] for d in mesh.devices.flat}
    return len(heights)


def rms_rows(wide, gain):
    scale = lax.rsqrt(jnp.mean(wide * wide, axis=-1, keepdims=True) + 1e-05)
    return wide * scale * gain


def project_kernel(
    holders, pieces, ids_ref, store_ref, gain_ref, wk_ref, wv_ref, all_ref, kv_ref, rows, load_sem, send_sem, recv_sem
):
    me = lax.axis_index("st")
    core = lax.axis_index("tp")
    piece = rows.shape[0] // pieces
    width = wk_ref.shape[1]
    length = kv_ref.shape[1]
    passages = piece // length

    def load(i):
        return pltpu.make_async_copy(
            store_ref.at[pl.ds(i * piece, piece)], rows.at[pl.ds(i * piece, piece)], load_sem.at[i]
        )

    for i in range(pieces):
        load(i).start()

    barrier = pltpu.get_barrier_semaphore()

    def other(step):
        return lax.rem(me + step, holders)

    def greet(step, carry):
        pl.semaphore_signal(barrier, inc=1, device_id=(other(step), core), device_id_type=MESH)
        return carry

    lax.fori_loop(1, holders, greet, 0)
    pl.semaphore_wait(barrier, holders - 1)

    def ids_copy(step):
        return pltpu.make_async_remote_copy(
            src_ref=ids_ref,
            dst_ref=all_ref.at[me],
            send_sem=send_sem.at[step],
            recv_sem=recv_sem.at[step],
            device_id=(other(step), core),
            device_id_type=MESH,
        )

    def send(step, carry):
        ids_copy(step).start()
        return carry

    lax.fori_loop(1, holders, send, 0)
    all_ref[me] = ids_ref[...]

    def project(i, carry):
        load(i).wait()
        start = pl.multiple_of(i * piece, piece)
        normed = rms_rows(rows[pl.ds(start, piece), :].astype(F32), gain_ref[...]).astype(BF16)
        for half, w_ref in enumerate((wk_ref, wv_ref)):
            part = jnp.dot(normed, w_ref[...], preferred_element_type=F32).astype(BF16)
            kv_ref[pl.ds(i * passages, passages), :, half * width : (half + 1) * width] = part.reshape(
                passages, length, width
            )
        return carry

    lax.fori_loop(0, pieces, project, 0)

    def finish(step, carry):
        ids_copy(step).wait()
        return carry

    lax.fori_loop(1, holders, finish, 0)


def project(ids, store, store_gain, w_key, w_value):
    holders = lax.axis_size("st")
    pass_dev, length, model = store.shape
    pieces = math.gcd(pass_dev, 6)
    width = w_key.shape[1]
    reads = ids.shape[0]
    padded = jnp.pad(ids.reshape(1, reads), ((0, 7), (0, 128 - reads)))
    return pl.pallas_call(
        functools.partial(project_kernel, holders, pieces),
        out_shape=(
            jax.ShapeDtypeStruct((holders, 8, 128), jnp.int32),
            jax.ShapeDtypeStruct((pass_dev, length, 2 * width), BF16),
        ),
        in_specs=[VMEM, ANY, VMEM, VMEM, VMEM],
        out_specs=(VMEM, VMEM),
        scratch_shapes=[
            pltpu.VMEM((pass_dev * length, model), BF16),
            pltpu.SemaphoreType.DMA((pieces,)),
            pltpu.SemaphoreType.DMA((holders,)),
            pltpu.SemaphoreType.DMA((holders,)),
        ],
        compiler_params=pltpu.CompilerParams(collective_id=0, has_side_effects=True, vmem_limit_bytes=LIMIT),
        cost_estimate=pl.CostEstimate(
            flops=4 * pass_dev * length * model * width, bytes_accessed=store.size * 2, transcendentals=0
        ),
    )(padded, store.reshape(pass_dev * length, model), store_gain.reshape(1, model), w_key, w_value)


def plan(ids, planes, pass_dev, most, caps):
    holders, reads = ids.shape
    side = holders // planes
    me = lax.axis_index("st")
    z, c = lax.div(me, side), lax.rem(me, side)
    i32 = jnp.int32
    everything = jnp.arange(holders * pass_dev, dtype=i32)
    need = jnp.any(ids.reshape(planes, side * reads, 1) == everything, axis=1)
    need = need.reshape(planes, planes, side, pass_dev)
    at = jnp.arange(planes, dtype=i32)
    ahead = (at[:, None] - at[None, :])[:, :, None, None]
    far = [jnp.max(jnp.where(need, jnp.maximum(sign * ahead, 0), 0), axis=0) for sign in (1, -1)]
    fits = []
    for way, reach in enumerate(far):
        for d in range(1, planes):
            count = jnp.sum((reach >= d).astype(i32), axis=2)
            left = [(planes - q - d) if way == 0 else (q - d + 1) for q in range(planes)]
            room = jnp.array([caps[k - 1] if k >= 1 else pass_dev for k in left], i32)
            fits.append(jnp.all(count <= room[:, None]))
    fits = jnp.all(jnp.stack(fits))

    lane = jnp.arange(pass_dev, dtype=i32)
    column = jnp.stack([lax.dynamic_index_in_dim(reach, c, axis=1, keepdims=False) for reach in far])
    before = (column[:, :, None, :] > column[:, :, :, None]) | (
        (column[:, :, None, :] == column[:, :, :, None]) & (lane[None, :] < lane[:, None])
    )
    place = jnp.sum(before.astype(i32), axis=3)
    own = lax.dynamic_index_in_dim(place, z, axis=1, keepdims=False)
    order = jnp.sum(jnp.where(own[:, None, :] == lane[None, :, None], lane, 0), axis=2)

    q = at[:, None]
    where_at = jnp.where(q == z, lane[None, :], jnp.where(q < z, place[0], place[1]))
    mine = lax.dynamic_slice_in_dim(ids, z * side, side, axis=0)
    holder = lax.div(mine, pass_dev)
    inside = mine - holder * pass_dev
    step = jnp.arange(reads, dtype=i32)
    earlier = (holder[:, None, :] == holder[:, :, None]) & (step[None, :] < step[:, None])
    rank = jnp.sum(earlier.astype(i32), axis=2)
    hq, hc = lax.div(holder, side), lax.rem(holder, side)
    flat = jnp.where(hc == c, hq * pass_dev + inside, -1)
    found = jnp.sum(
        jnp.where(
            flat[:, :, None] == jnp.arange(planes * pass_dev, dtype=i32), where_at.reshape(-1), 0
        ),
        axis=2,
    )
    target = jnp.where(hc == c, hq * most + rank, -1)
    pick = jnp.sum(
        jnp.where(target[:, None, :] == jnp.arange(planes * most, dtype=i32)[None, :, None], found[:, None, :], 0),
        axis=2,
    )
    slots = (hc * planes + hq) * most + rank
    slots = lax.dynamic_index_in_dim(slots, c, axis=0, keepdims=False)
    return fits, jnp.concatenate([order.reshape(-1), pick.reshape(-1), slots])


def chunks_of(caps):
    cut = [(0, caps[0] // 2, 1), (caps[0] // 2, caps[0], 1)]
    for k in range(1, len(caps)):
        if caps[k] > caps[k - 1]:
            cut.append((caps[k - 1], caps[k], k + 1))
    return cut


def mixer_kernel(
    planes,
    caps,
    most,
    block_len,
    tab,
    scale_ref,
    gain_ref,
    mix_ref,
    kv_hbm,
    hidden_hbm,
    w_pool_hbm,
    w_query_hbm,
    w_gate_hbm,
    w_branch_hbm,
    w_out_hbm,
    out_ref,
    kv,
    normed,
    w_pool,
    w_query,
    w_gate,
    w_branch,
    w_branch_far,
    w_out,
    w_out_far,
    pool_in,
    pool_out,
    pool_far,
    branch,
    gate,
    query,
    read,
    read_far,
    own_lists,
    *rest,
):
    reach = planes - 1
    lists = [rest[w * reach : (w + 1) * reach] for w in range(2)]
    picked, final, load_sem, z_send, z_recv, in_send, in_recv, core_send, core_recv = rest[2 * reach :]
    holders = lax.axis_size("st")
    side = holders // planes
    me = lax.axis_index("st")
    core = lax.axis_index("tp")
    z, c = lax.div(me, side), lax.rem(me, side)
    tokens, model = normed.shape
    half = out_ref.shape[1]
    pass_dev = kv.shape[0]
    cuts = chunks_of(caps)
    beyond = (planes - 1 - z, z)
    behind = (z, planes - 1 - z)
    step_to = (side, -side)

    mine = pl.ds(pl.multiple_of(core * half, half), half)
    theirs = pl.ds(pl.multiple_of((1 - core) * half, half), half)
    loads = [
        pltpu.make_async_copy(src, dst, load_sem.at[i])
        for i, (src, dst) in enumerate(
            (
                (kv_hbm, kv),
                (hidden_hbm, normed),
                (w_pool_hbm, w_pool),
                (w_query_hbm, w_query),
                (w_branch_hbm.at[:, mine], w_branch),
                (w_gate_hbm, w_gate),
                (w_out_hbm.at[:, mine], w_out),
            )
        )
    ]
    for copy in loads:
        copy.start()

    barrier = pltpu.get_barrier_semaphore()

    def greet(device):
        pl.semaphore_signal(barrier, inc=1, device_id=device, device_id_type=MESH)

    plane_mates = [z * side + lax.rem(c + rel, side) for rel in range(1, side)]
    for mate in plane_mates:
        greet((mate, core))
    greet((me, 1 - core))
    for way in range(2):
        pl.when(beyond[way] >= 1)(lambda way=way: greet((me + step_to[way], core)))
    pl.semaphore_wait(barrier, side + (z + reach - 1) // reach + (beyond[0] + reach - 1) // reach)

    def partner(src, dst, i):
        return pltpu.make_async_remote_copy(
            src_ref=src,
            dst_ref=dst,
            send_sem=core_send.at[i],
            recv_sem=core_recv.at[i],
            device_id=(me, 1 - core),
            device_id_type=MESH,
        )

    weight_swaps = [
        partner(w_branch_hbm.at[:, theirs], w_branch_far, 0),
        partner(w_out_hbm.at[:, theirs], w_out_far, 1),
    ]
    pool_swap = partner(pool_out, pool_far, 2)

    def hop(way, d, i):
        first, last, _ = cuts[i]
        src = own_lists.at[way] if d == 0 else lists[way][d - 1]
        return pltpu.make_async_remote_copy(
            src_ref=src.at[pl.ds(first, last - first)],
            dst_ref=lists[way][d].at[pl.ds(first, last - first)],
            send_sem=z_send.at[way, d, i],
            recv_sem=z_recv.at[way, d, i],
            device_id=(me + step_to[way], core),
            device_id_type=MESH,
        )

    def arrive(way, d, i):
        first, last, _ = cuts[i]
        ref = lists[way][d - 1].at[pl.ds(first, last - first)]
        pltpu.make_async_remote_copy(
            src_ref=ref,
            dst_ref=ref,
            send_sem=z_send.at[way, d - 1, i],
            recv_sem=z_recv.at[way, d - 1, i],
            device_id=(me, 1 - core),
            device_id_type=MESH,
        ).wait_recv()

    def forward(d, i):
        need = cuts[i][2]
        if need > reach - d:
            return
        for way in range(2):

            def go(way=way):
                arrive(way, d, i)
                hop(way, d, i).start()

            pl.when((behind[way] >= d) & (beyond[way] >= need))(go)

    def keep(d):
        for i, (_, _, need) in enumerate(cuts):
            if need > reach - d + 1:
                continue
            for way in range(2):
                pl.when((behind[way] >= d) & (beyond[way] + 1 == need))(lambda way=way, i=i: arrive(way, d, i))

    base = 2 * pass_dev

    def spread_copy(rel, q):
        mate = z * side + lax.rem(c + rel, side)
        return pltpu.make_async_remote_copy(
            src_ref=picked.at[rel - 1, pl.ds(q * most, most)],
            dst_ref=final.at[pl.ds((c * planes + q) * most, most)],
            send_sem=in_send.at[rel - 1, q],
            recv_sem=in_recv.at[c * planes + q],
            device_id=(mate, core),
            device_id_type=MESH,
        )

    def spread(src, q):
        for rel in range(1, side):
            mate = lax.rem(c + rel, side)
            for j in range(most):
                picked[rel - 1, q * most + j] = src[tab[base + (mate * planes + q) * most + j]]
        for rel in range(1, side):
            spread_copy(rel, q).start()
        for j in range(most):
            final[(c * planes + q) * most + j] = src[tab[base + (c * planes + q) * most + j]]

    def spread_from(d):
        for way in range(2):
            q = z - d if way == 0 else z + d
            pl.when(behind[way] >= d)(lambda way=way, q=q: spread(lists[way][d - 1], q))

    loads[0].wait()
    for way in range(2):
        for s in range(caps[-1]):
            own_lists[way, s] = kv[tab[way * pass_dev + s]]
    for i, (_, _, need) in enumerate(cuts):
        for way in range(2):
            pl.when(beyond[way] >= need)(lambda way=way, i=i: hop(way, 0, i).start())
    spread(kv, z)
    for copy in weight_swaps:
        copy.start()

    def norm(lo, hi, rows=32):
        def body(i, carry):
            at = pl.ds(pl.multiple_of(i * rows, rows), rows)
            normed[at, :] = rms_rows(normed[at, :].astype(F32), gain_ref[...]).astype(BF16)
            return carry

        lax.fori_loop(lo // rows, hi // rows, body, 0)

    piece = math.gcd(tokens, 256)
    pieces = tokens // piece
    halo = pool_in.shape[0] - tokens
    groups, group_dim = mix_ref.shape[:2]

    def project_rows(lo, hi):
        def body(i, carry):
            at = pl.ds(pl.multiple_of(i * piece, piece), piece)
            rows = normed[at, :]
            pool_in[pl.ds(pl.multiple_of(halo + i * piece, halo), piece), :] = jnp.dot(
                rows, w_pool[...], preferred_element_type=F32
            ).astype(BF16)
            query[at, :] = jnp.dot(rows, w_query[...], preferred_element_type=F32).astype(BF16)
            return carry

        lax.fori_loop(lo, hi, body, 0)

    def pool_rows(i, carry):
        at = pl.ds(pl.multiple_of(i * piece, piece), piece)
        position = i * piece + lax.broadcasted_iota(jnp.int32, (piece, 1), 0)
        for g in range(groups):
            cols = slice(g * group_dim, (g + 1) * group_dim)
            wide = pool_in[pl.ds(pl.multiple_of(i * piece, piece), piece + halo), cols].astype(F32)
            sums = []
            total = wide
            shift = 1
            while shift < halo:
                total = total + pltpu.roll(total, shift, 0)
                sums.append(total[halo:])
                shift *= 2
            per_core = [sums[k * groups + g] for k in range(len(sums) // groups)]
            level = per_core[0]
            window = 2 ** (g + 1)
            for k in range(1, len(per_core)):
                level = jnp.where(core == k, per_core[k], level)
                window = jnp.where(core == k, 2 ** (k * groups + g + 1), window)
            count = jnp.minimum(position + 1, window).astype(F32)
            pooled = (level / count - wide[halo:]).astype(BF16)
            pool_out[at, cols] = jnp.dot(pooled, mix_ref[g], preferred_element_type=F32).astype(BF16)
        return carry

    def gate_rows(lo, hi):
        def body(i, carry):
            at = pl.ds(pl.multiple_of(i * piece, piece), piece)
            for j in range(2):
                cols = slice(j * half // 2, (j + 1) * half // 2)
                logits = jnp.dot(normed[at, :], w_gate[:, cols], preferred_element_type=F32)
                gate[at, cols] = 1.0 / (1.0 + jnp.exp(-logits))
            return carry

        lax.fori_loop(lo, hi, body, 0)

    def two_terms(a, w, a_far, w_far):
        near = jnp.dot(a, w, preferred_element_type=F32).astype(BF16).astype(F32)
        far = jnp.dot(a_far, w_far, preferred_element_type=F32).astype(BF16).astype(F32)
        return near + far

    def branch_rows(i, carry):
        at = pl.ds(pl.multiple_of(i * piece, piece), piece)
        for j in range(2):
            cols = slice(j * half // 2, (j + 1) * half // 2)
            branch[at, cols] = two_terms(
                pool_out[at, :], w_branch[:, cols], pool_far[at, :], w_branch_far[:, cols]
            )
        return carry

    def forward_all(d, which):
        for i in which:
            if i < len(cuts):
                forward(d, i)

    loads[1].wait()
    norm(0, tokens)
    loads[2].wait()
    loads[3].wait()
    pool_in[:halo, :] = jnp.zeros((halo, pool_in.shape[1]), BF16)
    project_rows(0, pieces)
    forward_all(1, [0])
    lax.fori_loop(0, pieces, pool_rows, 0)
    pool_swap.start()
    loads[5].wait()
    gate_rows(0, pieces // 2)
    forward_all(1, [1])
    gate_rows(pieces // 2, pieces)
    loads[4].wait()
    loads[6].wait()
    for copy in weight_swaps:
        copy.wait()
    pool_swap.wait()
    lax.fori_loop(0, pieces, branch_rows, 0)
    forward_all(1, range(2, len(cuts)))
    keep(1)
    spread_from(1)
    for d in range(2, planes):
        if d < planes - 1:
            forward_all(d, range(len(cuts)))
        keep(d)
        spread_from(d)

    for rel in range(1, side):
        source = lax.rem(c + side - rel, side)
        for q in range(planes):
            at = pl.ds((source * planes + q) * most, most)
            pltpu.make_async_remote_copy(
                src_ref=final.at[at],
                dst_ref=final.at[at],
                send_sem=in_send.at[rel - 1, q],
                recv_sem=in_recv.at[source * planes + q],
                device_id=(me, 1 - core),
                device_id_type=MESH,
            ).wait_recv()

    blocks = tokens // block_len
    heads = scale_ref.shape[0]
    width = query.shape[1]
    head_dim = width // heads
    slot_base = base + side * planes * most
    per_block = (tab.shape[0] - slot_base) // blocks

    def read_swap(b):
        at = pl.ds(pl.multiple_of(b * block_len, block_len), block_len)
        return partner(read.at[at], read_far.at[at], 3 + b)

    def attend(b, carry):
        at = pl.ds(pl.multiple_of(b * block_len, block_len), block_len)
        memory = jnp.concatenate(
            [final[tab[slot_base + b * per_block + i]] for i in range(per_block)], axis=0
        )
        for h in range(heads):
            cut = slice(h * head_dim, (h + 1) * head_dim)
            scores = lax.dot_general(
                query[at, cut], memory[:, cut], (((1,), (1,)), ((), ())), preferred_element_type=F32
            )
            scores = scores * scale_ref[h]
            top = jnp.exp(scores - jnp.max(scores, axis=-1, keepdims=True))
            weights = (top * (1.0 / jnp.sum(top, axis=-1, keepdims=True))).astype(BF16)
            read[at, cut] = jnp.dot(
                weights, memory[:, width + h * head_dim : width + (h + 1) * head_dim], preferred_element_type=F32
            ).astype(BF16)
        read_swap(b).start()
        return carry

    lax.fori_loop(0, blocks, attend, 0)

    def finish(b, carry):
        at = pl.ds(pl.multiple_of(b * block_len, block_len), block_len)
        read_swap(b).wait()
        for j in range(2):
            cols = slice(j * half // 2, (j + 1) * half // 2)
            terms = two_terms(read[at, :], w_out[:, cols], read_far[at, :], w_out_far[:, cols])
            out_ref[at, cols] = (branch[at, cols] + gate[at, cols] * terms).astype(BF16)
        return carry

    lax.fori_loop(0, blocks, finish, 0)

    for way in range(2):
        for i, (_, _, need) in enumerate(cuts):
            for d in range(reach - need + 1):
                pl.when((behind[way] >= d) & (beyond[way] >= need))(
                    lambda way=way, d=d, i=i: hop(way, d, i).wait_send()
                )
    for rel in range(1, side):
        for q in range(planes):
            spread_copy(rel, q).wait_send()


def mixer(planes, caps, most, block_len, collective_id, operands):
    tab, scale, gain, mix, kv, hidden, w_pool, w_query, w_gate, w_branch, w_out = operands
    holders = lax.axis_size("st")
    side = holders // planes
    reach = planes - 1
    tokens, model = hidden.shape
    half = w_gate.shape[1]
    pool_width, width = w_pool.shape[1], w_query.shape[1]
    slot = kv.shape[1:]
    cores = lax.axis_size("tp")
    halo = 2 ** (cores * mix.shape[0])
    nch = len(chunks_of(caps))
    blocks = tokens // block_len
    v = pltpu.VMEM
    dma = pltpu.SemaphoreType.DMA
    flops = 2 * tokens * (model * (pool_width + width + half) + 2 * (pool_width + width) * half)
    return pl.pallas_call(
        functools.partial(mixer_kernel, planes, caps, most, block_len),
        out_shape=jax.ShapeDtypeStruct((tokens, half), BF16),
        in_specs=[SMEM, SMEM, VMEM, VMEM] + [ANY] * 7,
        out_specs=VMEM,
        scratch_shapes=[
            v(kv.shape, BF16),
            v(hidden.shape, BF16),
            v(w_pool.shape, BF16),
            v(w_query.shape, BF16),
            v(w_gate.shape, BF16),
            v((pool_width, half), BF16),
            v((pool_width, half), BF16),
            v((width, half), BF16),
            v((width, half), BF16),
            v((tokens + halo, pool_width), BF16),
            v((tokens, pool_width), BF16),
            v((tokens, pool_width), BF16),
            v((tokens, half), F32),
            v((tokens, half), F32),
            v((tokens, width), BF16),
            v((tokens, width), BF16),
            v((tokens, width), BF16),
            v((2, caps[-1], *slot), BF16),
            *[v((caps[reach - d], *slot), BF16) for _ in range(2) for d in range(1, planes)],
            v((side - 1, planes * most, *slot), BF16),
            v((holders * most, *slot), BF16),
            dma((7,)),
            dma((2, reach, nch)),
            dma((2, reach, nch)),
            dma((side - 1, planes)),
            dma((holders,)),
            dma((3 + blocks,)),
            dma((3 + blocks,)),
        ],
        compiler_params=pltpu.CompilerParams(
            collective_id=collective_id, has_side_effects=True, vmem_limit_bytes=LIMIT
        ),
        cost_estimate=pl.CostEstimate(flops=flops, bytes_accessed=32 * 2**20, transcendentals=0),
    )(*operands)


def body(
    planes,
    hidden,
    norm_gain,
    store,
    store_gain,
    passage_ids,
    w_pool,
    pool_mix,
    w_branch,
    w_query,
    w_key,
    w_value,
    sharpness,
    w_out,
    w_gate,
):
    holders = lax.axis_size("st")
    side = holders // planes
    blocks, per_block = passage_ids.shape
    reads = blocks * per_block
    pass_dev = store.shape[0]
    tokens, model = hidden.shape
    most = max(1, 2 * reads // holders)
    head_dim = w_query.shape[1] // sharpness.shape[0]

    all_ids, own_kv = project(passage_ids.reshape(-1), store, store_gain, w_key, w_value)
    one = min(pass_dev, side * most)
    full = tuple(min(pass_dev, k * one) for k in range(1, planes))
    short = tuple(min(f, (11 * one) // 16 + (k > 0) * pass_dev // 6 + (k > 1) * pass_dev // 12) for k, f in enumerate(full))
    fits, tab = plan(all_ids[:, 0, :reads], planes, pass_dev, most, short)
    operands = (
        tab,
        sharpness / math.sqrt(head_dim),
        norm_gain.reshape(1, model),
        pool_mix,
        own_kv,
        hidden,
        w_pool,
        w_query,
        w_gate,
        w_branch,
        w_out,
    )
    run = functools.partial(mixer, planes)
    block_len = tokens // blocks
    return lax.cond(
        fits,
        lambda *ops: run(short, most, block_len, 1, ops),
        lambda *ops: run(full, most, block_len, 2, ops),
        *operands,
    )


def solution(mesh):
    placed = (
        P("st", None),
        P(),
        P("st", None, None),
        P(),
        P("st", None),
        P(None, "tp"),
        P("tp", None, None),
        P("tp", None),
        P(None, "tp"),
        P(None, "tp"),
        P(None, "tp"),
        P("tp"),
        P("tp", None),
        P(None, "tp"),
    )
    return jax.shard_map(
        functools.partial(body, planes_of(mesh)), mesh=mesh, in_specs=placed, out_specs=P("st", "tp"), check_vma=False
    )
```

time: 140 us -> 106 us (0.76)
  Pallas kernels: 4.83 us -> 86.8 us
  waiting for transfers between devices: 49.6 us -> 0 us
  matrix products: 47.2 us -> 0 us
  starting transfers between devices: 17 us -> 0 us
  other arithmetic: 10.5 us -> 6.64 us
  between operations: 0.29 us -> 3.93 us
  local copies, waits for them, and re-layouts: 10.3 us -> 6.96 us
    pallas_call x1 -> x2, Pallas kernels: 4.83 us -> 86.8 us  [the longest x1 74.7 us: mixer(): pl.pallas_call(functools.partial(mixer_kernel, planes, caps, most, block_...]
    all_to_all x2 -> x0, waiting for transfers between devices: 49.6 us -> none  [the longest x1 49.6 us: body(): kv = lax.all_to_all(packed, 'st', split_axis=0, concat_axis=0, tiled=True)]
    dot_general x9 -> x0, matrix products: 47.2 us -> none  [the longest x1 18.1 us: pool_branch(): jnp.einsum('tgc,gcd->tgd', pooled, pool_mix, preferred_element_type=jnp.f...]
    all_to_all x2 -> x0, starting transfers between devices: 13.1 us -> none  [the longest x1 6.61 us: body(): lax.all_to_all(request, 'st', split_axis=0, concat_axis=0, tiled=True)]
    reduce_sum x4 -> x7, other arithmetic: 7.57 us -> 1.58 us  [the longest x2 0.57 us: plan(): count = jnp.sum((reach >= d).astype(i32), axis=2)]
    gather x1 -> x0, local copies, waits for them, and re-layouts: 4.2 us -> none  [body(): packed = own_kv[incoming.reshape(-1)]]
    reduce_and x0 -> x6, other arithmetic: none -> 3.93 us  [plan(): fits.append(jnp.all(count <= room[:, None]))]
    ppermute x4 -> x0, starting transfers between devices: 3.9 us -> none  [swap(): return lax.ppermute(array, 'tp', [(0, 1), (1, 0)])]
  transfers between devices with their start and end apart: 6 -> 0, of which waited for: 1 -> 0; matrix products, arithmetic and copies ran while one was open for 40% -> 0% of each run, Pallas kernels for 3% -> 0%
where the time goes in v1:
time: 106 us; the launch traced here: 105 us
  Pallas kernels  86.8 us (82%)
  local copies, waits for them, and re-layouts  6.96 us (7%)
  other arithmetic  6.64 us (6%)
  between operations  3.93 us (4%)
    pallas_call x1, Pallas kernels, mixer(): pl.pallas_call(functools.partial(mixer_kernel, planes, caps, most, block_...  74.7 us
    pallas_call x1, Pallas kernels, project(): pl.pallas_call(functools.partial(project_kernel, holders, pieces), out_sh...  12.1 us
    unnamed x24, local copies, waits for them, and re-layouts  4.45 us
    reduce_and x6, other arithmetic, plan(): fits.append(jnp.all(count <= room[:, None]))  3.93 us

profile of v1, /device:TPU:13, one launch (start us, length us, event | category | flops | bytes accessed | tf_op | source)
XLA Modules:
  0.0 104.5 jit_solution(13899723662406283304)
XLA Ops:
  0.0 0.7 broadcast_multiply_fusion
  1.1 0.8 copy.29
  1.9 0.6 pad.4.ids_ref
  2.6 12.1 %shard_map.192 = (s32[16,8,128]{2,1,0:T(8,128)}, bf16[24,64,512]{2,1,0:T(8,128)(2,1)}) custom-call(s32[8,128]{1,0:T(8,128)} %pad.4.ids_ref, bf16[1536,2048]{1,0:T(8,128)(2,1)} %bitcast.22, f32[1,2048]{1,0:T(1,128)} %bitcast.23, bf16[2048,256]{1,0:T(8,128)(2,1)} %wk_ref.1, bf16[2048,256]{1,0:T(8,128)(2,1)} %wv_ref.1), custom_call_target="tpu_custom_call" | custom-call | flops 3221225472 | bytes 6291456 | tf_op jit(solution)/shard_map/pallas_call | solution.py:104
  14.7 0.9 fusion.3
  15.6 0.2 convert_reduce_fusion.1
  16.0 0.2 fusion
  16.2 0.1 reduce_or.12
  16.3 0.1 select_reduce_fusion.2
  16.4 0.3 convert_reduce_fusion.2
  16.8 0.7 compare_reduce_fusion
  17.5 0.3 convert_reduce_fusion.5
  17.9 0.6 compare_reduce_fusion.3
  18.5 0.3 convert_reduce_fusion
  18.9 0.1 select_reduce_fusion.4
  19.2 0.2 select_reduce_fusion
  19.5 0.2 select_reduce_fusion.1
  19.9 0.7 compare_reduce_fusion.4
  20.7 0.6 compare_reduce_fusion.5
  23.2 0.6 compare_reduce_fusion.1
  24.0 0.6 compare_reduce_fusion.2
  26.5 74.9 %conditional.1 = (bf16[1024,1024]{1,0:T(8,128)(2,1)}) conditional(s32[]{:T(128)} %convert_element_type.33, (s32[144]{0:T(256)S(1)}, f32[2]{0:T(128)S(1)}, f32[1,2048]{1,0:T(1,128)S(1)}, bf16[2,256,256]{2,1,0:T(8,128)(2,1)S(1)}, bf16[24,64,512]{2,1,0:T(8,128)(2,1)}, /*index=5*/bf16[1024,2048]{1,0:T(8,128)(2,1)}, bf16[2048,512]{1,0:T(8,128)(2,1)}, ...), branch_computations={%region_20.21_spmd, %region_21.22_spmd} | conditional | flops 10737418240 | bytes 33554440 | solution.py:650
  26.5 74.7 %branch_1_fun.1 = bf16[1024,1024]{1,0:T(8,128)(2,1)} custom-call(s32[144]{0:T(256)S(1)} %get-tuple-element.63.tab, f32[2]{0:T(128)S(1)} %get-tuple-element.64.scale_ref, f32[1,2048]{1,0:T(1,128)S(1)} %get-tuple-element.65.gain_ref, bf16[2,256,256]{2,1,0:T(8,128)(2,1)S(1)} %get-tuple-element.66.mix_ref, bf16[24,64,512]{2,1,0:T(8,128)(2,1)} %get-tuple-element.67.kv_hbm, ...), custom_call_target="tpu_custom_call" | custom-call | flops 10737418240 | bytes 33554432 | tf_op jit(solution)/shard_map/cond/branch_1_fun/pallas_call | solution.py:562
  101.5 3.1 %copy.46 = bf16[1024,1024]{1,0:T(8,128)(2,1)} copy(bf16[1024,1024]{1,0:T(8,128)(2,1)} %get-tuple-element.78) | data formatting | bytes 4194304
  (50 shorter events, 1.7 us)
Async XLA Ops:
  2.5 14.2 %copy-start.5 = (s32[4]{0:T(128)S(1)}, s32[4]{0:T(128)}, u32[]{:S(2)}) copy-start(s32[4]{0:T(128)} %constant.74.clone) | copy-start | bytes 52
  2.6 15.3 %copy-start.4 = (s32[4]{0:T(128)S(1)}, s32[4]{0:T(128)}, u32[]{:S(2)}) copy-start(s32[4]{0:T(128)} %constant.71.clone) | copy-start | bytes 52
  2.6 17.3 %copy-start.3 = (s32[4]{0:T(128)S(1)}, s32[4]{0:T(128)}, u32[]{:S(2)}) copy-start(s32[4]{0:T(128)} %constant.70.clone) | copy-start | bytes 52
  2.6 18.1 %copy-start.2 = (s32[4]{0:T(128)S(1)}, s32[4]{0:T(128)}, u32[]{:S(2)}) copy-start(s32[4]{0:T(128)} %constant.69.clone) | copy-start | bytes 52
  2.6 20.6 %copy-start.1 = (s32[4]{0:T(128)S(1)}, s32[4]{0:T(128)}, u32[]{:S(2)}) copy-start(s32[4]{0:T(128)} %constant.73.clone) | copy-start | bytes 52
  2.6 21.3 %copy-start = (s32[4]{0:T(128)S(1)}, s32[4]{0:T(128)}, u32[]{:S(2)}) copy-start(s32[4]{0:T(128)} %constant.72.clone) | copy-start | bytes 52
  2.6 23.9 %copy-start.6 = (bf16[2,256,256]{2,1,0:T(8,128)(2,1)S(1)}, bf16[2,256,256]{2,1,0:T(8,128)(2,1)}, u32[]{:S(2)}) copy-start(bf16[2,256,256]{2,1,0:T(8,128)(2,1)} %param.28) | copy-start | bytes 786436
  2.6 23.9 %copy-start.7 = (f32[2048]{0:T(1024)S(1)}, f32[2048]{0:T(1024)}, u32[]{:S(2)}) copy-start(f32[2048]{0:T(1024)} %param.23) | copy-start | bytes 24580

commit v2 on v1

--- a/solution.py
+++ b/solution.py
@@ -27,15 +27,144 @@
     return wide * scale * gain
 
 
+def plan_tables(holders, planes, reads, pass_dev, most, variants, all_ref, tab_ref):
+    side = holders // planes
+    lanes = 128
+    per = lanes // reads
+    me = lax.axis_index("st")
+    z, c = lax.div(me, side), lax.rem(me, side)
+
+    def lane_of(rows):
+        return lax.broadcasted_iota(jnp.int32, (rows, lanes), 1).astype(F32)
+
+    def sub_of(rows, width=lanes):
+        return lax.broadcasted_iota(jnp.int32, (rows, width), 0).astype(F32)
+
+    def whole(x, by):
+        return jnp.floor((x + 0.5) * (1.0 / by))
+
+    segment = whole(lane_of(1), reads)
+
+    def requests(plane):
+        return [requests_row(all_ref, plane, side, per, r, segment) for r in range(side // per)]
+
+    holder_at = lax.broadcasted_iota(jnp.int32, (1, holders), 1).astype(F32)
+    plane_at = whole(holder_at, side)
+    far_up = jnp.zeros((pass_dev, holders), F32)
+    far_down = jnp.zeros((pass_dev, holders), F32)
+    for p in range(planes):
+        hits = jnp.zeros((pass_dev, holders), F32)
+        for row in requests(p):
+            owner = whole(row, pass_dev)
+            inside = row - owner * pass_dev
+            a = jnp.where(inside == sub_of(pass_dev), 1.0, 0.0).astype(BF16)
+            b = jnp.where(owner == sub_of(holders), 1.0, 0.0).astype(BF16)
+            hits = hits + lax.dot_general(a, b, (((1,), (1,)), ((), ())), preferred_element_type=F32)
+        ahead = jnp.where(hits > 0.5, p - plane_at, 0.0)
+        far_up = jnp.maximum(far_up, ahead)
+        far_down = jnp.maximum(far_down, -ahead)
+
+    longest = [jnp.zeros((1, holders), F32) for _ in range(planes - 1)]
+    for reach, left in ((far_up, planes - 1 - plane_at), (far_down, plane_at)):
+        for d in range(1, planes):
+            count = jnp.sum(jnp.where(reach >= d, 1.0, 0.0), axis=0, keepdims=True)
+            for k in range(planes - 1):
+                longest[k] = jnp.maximum(longest[k], jnp.where(left - d == k, count, 0.0))
+    longest = [jnp.max(x, axis=1, keepdims=True) for x in longest]
+    variant = jnp.zeros((1, 1), F32)
+    for caps in variants[:-1]:
+        over = jnp.zeros((1, 1), F32)
+        for k, room in enumerate(caps):
+            over = jnp.maximum(over, jnp.where(longest[k] > room, 1.0, 0.0))
+        variant = variant + over
+
+    lower = lax.broadcasted_iota(jnp.int32, (pass_dev, pass_dev), 1) < lax.broadcasted_iota(
+        jnp.int32, (pass_dev, pass_dev), 0
+    )
+    diagonal = lax.broadcasted_iota(jnp.int32, (pass_dev, pass_dev), 1) == lax.broadcasted_iota(
+        jnp.int32, (pass_dev, pass_dev), 0
+    )
+
+    def place_in(reach, q):
+        col = jnp.sum(jnp.where(holder_at == (q * side + c).astype(F32), reach, 0.0), axis=1, keepdims=True)
+        row = jnp.sum(jnp.where(diagonal, col, 0.0), axis=0, keepdims=True)
+        before = (row > col) | ((row == col) & lower)
+        return jnp.sum(jnp.where(before, 1.0, 0.0), axis=1, keepdims=True)
+
+    number = sub_of(pass_dev)
+    orders = [
+        jnp.sum(jnp.where(place_in(reach, z) == lane_of(pass_dev), number, 0.0), axis=0, keepdims=True)
+        for reach in (far_up, far_down)
+    ]
+    where_at = []
+    for q in range(planes):
+        place = place_in(jnp.where(q < z, far_up, far_down), jnp.int32(q))
+        where_at.append(jnp.where(q == z, sub_of(pass_dev, 1), place))
+
+    square_sub = sub_of(lanes)
+    square_lane = lane_of(lanes)
+    close = (square_sub < square_lane) & (whole(square_sub, reads) == whole(square_lane, reads))
+    picks = jnp.zeros((planes * most, lanes), F32)
+    slots = jnp.zeros((1, lanes), F32)
+    for r, row in enumerate(requests(z)):
+        owner = whole(row, pass_dev)
+        inside = row - owner * pass_dev
+        owner_col = jnp.sum(jnp.where(square_sub == square_lane, owner, 0.0), axis=1, keepdims=True)
+        rank = jnp.sum(jnp.where(close & (owner_col == owner), 1.0, 0.0), axis=0, keepdims=True)
+        of_plane = whole(owner, side)
+        of_side = owner - of_plane * side
+        here = of_side == c.astype(F32)
+        found = jnp.zeros((1, lanes), F32)
+        for q in range(planes):
+            hit = here & (of_plane == q) & (inside == number)
+            found = found + jnp.sum(jnp.where(hit, where_at[q], 0.0), axis=0, keepdims=True)
+        target = jnp.where(here, of_plane * most + rank, -1.0)
+        values = jnp.where(target == sub_of(planes * most), found, 0.0)
+        for t in range(per):
+            column = jnp.sum(jnp.where(segment == t, values, 0.0), axis=1, keepdims=True)
+            picks = jnp.where(lane_of(planes * most) == r * per + t, column, picks)
+        slots = jnp.where(lax.div(c, per) == r, (of_side * planes + of_plane) * most + rank, slots)
+    for i, row in enumerate((*orders, slots, variant + jnp.zeros((1, lanes), F32))):
+        tab_ref[i : i + 1, :] = row.astype(jnp.int32)
+    tab_ref[8 : 8 + planes * most, :] = picks.astype(jnp.int32)
+
+
+def requests_row(all_ref, plane, side, per, r, segment):
+    row = jnp.zeros(segment.shape, F32)
+    for t in range(per):
+        ids = all_ref[plane * side + r * per + t][0:1, :].astype(F32)
+        row = jnp.where(segment == t, ids, row)
+    return row
+
+
 def project_kernel(
-    holders, pieces, ids_ref, store_ref, gain_ref, wk_ref, wv_ref, all_ref, kv_ref, rows, load_sem, send_sem, recv_sem
+    holders,
+    planes,
+    pieces,
+    most,
+    variants,
+    ids_ref,
+    store_ref,
+    gain_ref,
+    wk_ref,
+    wv_ref,
+    tab_ref,
+    kv_ref,
+    rows,
+    mine_ids,
+    all_ref,
+    load_sem,
+    send_sem,
+    recv_sem,
 ):
     me = lax.axis_index("st")
     core = lax.axis_index("tp")
     piece = rows.shape[0] // pieces
     width = wk_ref.shape[1]
-    length = kv_ref.shape[1]
+    pass_dev, length, _ = kv_ref.shape
     passages = piece // length
+    blocks, per_block = ids_ref.shape
+    reads = blocks * per_block
 
     def load(i):
         return pltpu.make_async_copy(
@@ -55,24 +184,18 @@
         return carry
 
     lax.fori_loop(1, holders, greet, 0)
-    pl.semaphore_wait(barrier, holders - 1)
-
-    def ids_copy(step):
-        return pltpu.make_async_remote_copy(
-            src_ref=ids_ref,
-            dst_ref=all_ref.at[me],
-            send_sem=send_sem.at[step],
-            recv_sem=recv_sem.at[step],
-            device_id=(other(step), core),
-            device_id_type=MESH,
-        )
-
-    def send(step, carry):
-        ids_copy(step).start()
-        return carry
-
-    lax.fori_loop(1, holders, send, 0)
-    all_ref[me] = ids_ref[...]
+
+    lane = lax.broadcasted_iota(jnp.int32, (blocks, 128), 1)
+    lane = lane - reads * jnp.floor((lane.astype(F32) + 0.5) * (1.0 / reads)).astype(jnp.int32)
+    block = jnp.floor((lane.astype(F32) + 0.5) * (1.0 / per_block)).astype(jnp.int32)
+    inner = lane - block * per_block
+    spread_ids = jnp.zeros((blocks, 128), F32)
+    for k in range(per_block):
+        spread_ids = jnp.where(inner == k, ids_ref[:, k : k + 1].astype(F32), spread_ids)
+    at_block = lax.broadcasted_iota(jnp.int32, (blocks, 128), 0) == block
+    row = jnp.sum(jnp.where(at_block, spread_ids, 0.0), axis=0, keepdims=True)
+    mine_ids[...] = jnp.broadcast_to(row, mine_ids.shape).astype(jnp.int32)
+    all_ref[me] = jnp.broadcast_to(row, mine_ids.shape).astype(jnp.int32)
 
     def project(i, carry):
         load(i).wait()
@@ -85,32 +208,58 @@
             )
         return carry
 
-    lax.fori_loop(0, pieces, project, 0)
+    first = pieces // 2
+    with jax.named_scope("kv0"):
+        lax.fori_loop(0, first, project, 0)
+    with jax.named_scope("greet_all"):
+        pl.semaphore_wait(barrier, holders - 1)
+
+    def ids_copy(step):
+        return pltpu.make_async_remote_copy(
+            src_ref=mine_ids,
+            dst_ref=all_ref.at[me],
+            send_sem=send_sem.at[step],
+            recv_sem=recv_sem.at[step],
+            device_id=(other(step), core),
+            device_id_type=MESH,
+        )
+
+    def send(step, carry):
+        ids_copy(step).start()
+        return carry
+
+    lax.fori_loop(1, holders, send, 0)
+    with jax.named_scope("kv1"):
+        lax.fori_loop(first, pieces, project, 0)
 
     def finish(step, carry):
         ids_copy(step).wait()
         return carry
 
-    lax.fori_loop(1, holders, finish, 0)
-
-
-def project(ids, store, store_gain, w_key, w_value):
+    with jax.named_scope("ids"):
+        lax.fori_loop(1, holders, finish, 0)
+    with jax.named_scope("tables"):
+        plan_tables(holders, planes, reads, pass_dev, most, variants, all_ref, tab_ref)
+
+
+def project(planes, most, variants, ids, store, store_gain, w_key, w_value):
     holders = lax.axis_size("st")
     pass_dev, length, model = store.shape
     pieces = math.gcd(pass_dev, 6)
     width = w_key.shape[1]
-    reads = ids.shape[0]
-    padded = jnp.pad(ids.reshape(1, reads), ((0, 7), (0, 128 - reads)))
+    table_rows = 8 + -(-planes * most // 8) * 8
     return pl.pallas_call(
-        functools.partial(project_kernel, holders, pieces),
+        functools.partial(project_kernel, holders, planes, pieces, most, variants),
         out_shape=(
-            jax.ShapeDtypeStruct((holders, 8, 128), jnp.int32),
+            jax.ShapeDtypeStruct((table_rows, 128), jnp.int32),
             jax.ShapeDtypeStruct((pass_dev, length, 2 * width), BF16),
         ),
         in_specs=[VMEM, ANY, VMEM, VMEM, VMEM],
         out_specs=(VMEM, VMEM),
         scratch_shapes=[
             pltpu.VMEM((pass_dev * length, model), BF16),
+            pltpu.VMEM((8, 128), jnp.int32),
+            pltpu.VMEM((holders, 8, 128), jnp.int32),
             pltpu.SemaphoreType.DMA((pieces,)),
             pltpu.SemaphoreType.DMA((holders,)),
             pltpu.SemaphoreType.DMA((holders,)),
@@ -119,63 +268,7 @@
         cost_estimate=pl.CostEstimate(
             flops=4 * pass_dev * length * model * width, bytes_accessed=store.size * 2, transcendentals=0
         ),
-    )(padded, store.reshape(pass_dev * length, model), store_gain.reshape(1, model), w_key, w_value)
-
-
-def plan(ids, planes, pass_dev, most, caps):
-    holders, reads = ids.shape
-    side = holders // planes
-    me = lax.axis_index("st")
-    z, c = lax.div(me, side), lax.rem(me, side)
-    i32 = jnp.int32
-    everything = jnp.arange(holders * pass_dev, dtype=i32)
-    need = jnp.any(ids.reshape(planes, side * reads, 1) == everything, axis=1)
-    need = need.reshape(planes, planes, side, pass_dev)
-    at = jnp.arange(planes, dtype=i32)
-    ahead = (at[:, None] - at[None, :])[:, :, None, None]
-    far = [jnp.max(jnp.where(need, jnp.maximum(sign * ahead, 0), 0), axis=0) for sign in (1, -1)]
-    fits = []
-    for way, reach in enumerate(far):
-        for d in range(1, planes):
-            count = jnp.sum((reach >= d).astype(i32), axis=2)
-            left = [(planes - q - d) if way == 0 else (q - d + 1) for q in range(planes)]
-            room = jnp.array([caps[k - 1] if k >= 1 else pass_dev for k in left], i32)
-            fits.append(jnp.all(count <= room[:, None]))
-    fits = jnp.all(jnp.stack(fits))
-
-    lane = jnp.arange(pass_dev, dtype=i32)
-    column = jnp.stack([lax.dynamic_index_in_dim(reach, c, axis=1, keepdims=False) for reach in far])
-    before = (column[:, :, None, :] > column[:, :, :, None]) | (
-        (column[:, :, None, :] == column[:, :, :, None]) & (lane[None, :] < lane[:, None])
-    )
-    place = jnp.sum(before.astype(i32), axis=3)
-    own = lax.dynamic_index_in_dim(place, z, axis=1, keepdims=False)
-    order = jnp.sum(jnp.where(own[:, None, :] == lane[None, :, None], lane, 0), axis=2)
-
-    q = at[:, None]
-    where_at = jnp.where(q == z, lane[None, :], jnp.where(q < z, place[0], place[1]))
-    mine = lax.dynamic_slice_in_dim(ids, z * side, side, axis=0)
-    holder = lax.div(mine, pass_dev)
-    inside = mine - holder * pass_dev
-    step = jnp.arange(reads, dtype=i32)
-    earlier = (holder[:, None, :] == holder[:, :, None]) & (step[None, :] < step[:, None])
-    rank = jnp.sum(earlier.astype(i32), axis=2)
-    hq, hc = lax.div(holder, side), lax.rem(holder, side)
-    flat = jnp.where(hc == c, hq * pass_dev + inside, -1)
-    found = jnp.sum(
-        jnp.where(
-            flat[:, :, None] == jnp.arange(planes * pass_dev, dtype=i32), where_at.reshape(-1), 0
-        ),
-        axis=2,
-    )
-    target = jnp.where(hc == c, hq * most + rank, -1)
-    pick = jnp.sum(
-        jnp.where(target[:, None, :] == jnp.arange(planes * most, dtype=i32)[None, :, None], found[:, None, :], 0),
-        axis=2,
-    )
-    slots = (hc * planes + hq) * most + rank
-    slots = lax.dynamic_index_in_dim(slots, c, axis=0, keepdims=False)
-    return fits, jnp.concatenate([order.reshape(-1), pick.reshape(-1), slots])
+    )(ids, store.reshape(pass_dev * length, model), store_gain.reshape(1, model), w_key, w_value)
 
 
 def chunks_of(caps):
@@ -191,6 +284,7 @@
     caps,
     most,
     block_len,
+    per_block,
     tab,
     scale_ref,
     gain_ref,
@@ -233,7 +327,6 @@
     z, c = lax.div(me, side), lax.rem(me, side)
     tokens, model = normed.shape
     half = out_ref.shape[1]
-    pass_dev = kv.shape[0]
     cuts = chunks_of(caps)
     beyond = (planes - 1 - z, z)
     behind = (z, planes - 1 - z)
@@ -269,7 +362,8 @@
     greet((me, 1 - core))
     for way in range(2):
         pl.when(beyond[way] >= 1)(lambda way=way: greet((me + step_to[way], core)))
-    pl.semaphore_wait(barrier, side + (z + reach - 1) // reach + (beyond[0] + reach - 1) // reach)
+    with jax.named_scope("greet"):
+        pl.semaphore_wait(barrier, side + (z + reach - 1) // reach + (beyond[0] + reach - 1) // reach)
 
     def partner(src, dst, i):
         return pltpu.make_async_remote_copy(
@@ -330,7 +424,6 @@
             for way in range(2):
                 pl.when((behind[way] >= d) & (beyond[way] + 1 == need))(lambda way=way, i=i: arrive(way, d, i))
 
-    base = 2 * pass_dev
 
     def spread_copy(rel, q):
         mate = z * side + lax.rem(c + rel, side)
@@ -347,27 +440,28 @@
         for rel in range(1, side):
             mate = lax.rem(c + rel, side)
             for j in range(most):
-                picked[rel - 1, q * most + j] = src[tab[base + (mate * planes + q) * most + j]]
+                picked[rel - 1, q * most + j] = src[tab[8 + q * most + j, mate]]
         for rel in range(1, side):
             spread_copy(rel, q).start()
         for j in range(most):
-            final[(c * planes + q) * most + j] = src[tab[base + (c * planes + q) * most + j]]
+            final[(c * planes + q) * most + j] = src[tab[8 + q * most + j, c]]
 
     def spread_from(d):
         for way in range(2):
             q = z - d if way == 0 else z + d
             pl.when(behind[way] >= d)(lambda way=way, q=q: spread(lists[way][d - 1], q))
 
-    loads[0].wait()
-    for way in range(2):
-        for s in range(caps[-1]):
-            own_lists[way, s] = kv[tab[way * pass_dev + s]]
-    for i, (_, _, need) in enumerate(cuts):
+    with jax.named_scope("first_sends"):
+        loads[0].wait()
         for way in range(2):
-            pl.when(beyond[way] >= need)(lambda way=way, i=i: hop(way, 0, i).start())
-    spread(kv, z)
-    for copy in weight_swaps:
-        copy.start()
+            for s in range(caps[-1]):
+                own_lists[way, s] = kv[tab[way, s]]
+        for i, (_, _, need) in enumerate(cuts):
+            for way in range(2):
+                pl.when(beyond[way] >= need)(lambda way=way, i=i: hop(way, 0, i).start())
+        spread(kv, z)
+        for copy in weight_swaps:
+            copy.start()
 
     def norm(lo, hi, rows=32):
         def body(i, carry):
@@ -448,78 +542,95 @@
             if i < len(cuts):
                 forward(d, i)
 
-    loads[1].wait()
-    norm(0, tokens)
-    loads[2].wait()
-    loads[3].wait()
-    pool_in[:halo, :] = jnp.zeros((halo, pool_in.shape[1]), BF16)
-    project_rows(0, pieces)
-    forward_all(1, [0])
-    lax.fori_loop(0, pieces, pool_rows, 0)
-    pool_swap.start()
-    loads[5].wait()
-    gate_rows(0, pieces // 2)
-    forward_all(1, [1])
-    gate_rows(pieces // 2, pieces)
-    loads[4].wait()
-    loads[6].wait()
-    for copy in weight_swaps:
-        copy.wait()
-    pool_swap.wait()
-    lax.fori_loop(0, pieces, branch_rows, 0)
-    forward_all(1, range(2, len(cuts)))
-    keep(1)
-    spread_from(1)
+    with jax.named_scope("norm"):
+        loads[1].wait()
+        norm(0, tokens)
+    with jax.named_scope("project"):
+        loads[2].wait()
+        loads[3].wait()
+        pool_in[:halo, :] = jnp.zeros((halo, pool_in.shape[1]), BF16)
+        project_rows(0, pieces)
+    with jax.named_scope("pool"):
+        forward_all(1, [0])
+        lax.fori_loop(0, pieces, pool_rows, 0)
+        pool_swap.start()
+    with jax.named_scope("gate"):
+        loads[5].wait()
+        gate_rows(0, pieces // 2)
+        forward_all(1, [1])
+        gate_rows(pieces // 2, pieces)
+    with jax.named_scope("branch"):
+        loads[4].wait()
+        loads[6].wait()
+        for copy in weight_swaps:
+            copy.wait()
+        pool_swap.wait()
+        lax.fori_loop(0, pieces, branch_rows, 0)
+    with jax.named_scope("spread1"):
+        forward_all(1, range(2, len(cuts)))
+        keep(1)
+        spread_from(1)
     for d in range(2, planes):
-        if d < planes - 1:
-            forward_all(d, range(len(cuts)))
-        keep(d)
-        spread_from(d)
-
-    for rel in range(1, side):
-        source = lax.rem(c + side - rel, side)
-        for q in range(planes):
-            at = pl.ds((source * planes + q) * most, most)
-            pltpu.make_async_remote_copy(
-                src_ref=final.at[at],
-                dst_ref=final.at[at],
-                send_sem=in_send.at[rel - 1, q],
-                recv_sem=in_recv.at[source * planes + q],
-                device_id=(me, 1 - core),
-                device_id_type=MESH,
-            ).wait_recv()
+        with jax.named_scope(f"spread{d}"):
+            if d < planes - 1:
+                forward_all(d, range(len(cuts)))
+            keep(d)
+            spread_from(d)
+
+    with jax.named_scope("arrivals"):
+        for rel in range(1, side):
+            source = lax.rem(c + side - rel, side)
+            for q in range(planes):
+                at = pl.ds((source * planes + q) * most, most)
+                pltpu.make_async_remote_copy(
+                    src_ref=final.at[at],
+                    dst_ref=final.at[at],
+                    send_sem=in_send.at[rel - 1, q],
+                    recv_sem=in_recv.at[source * planes + q],
+                    device_id=(me, 1 - core),
+                    device_id_type=MESH,
+                ).wait_recv()
 
     blocks = tokens // block_len
     heads = scale_ref.shape[0]
     width = query.shape[1]
     head_dim = width // heads
-    slot_base = base + side * planes * most
-    per_block = (tab.shape[0] - slot_base) // blocks
+    reads = blocks * per_block
+    slot_base = lax.rem(c, 128 // reads) * reads
 
     def read_swap(b):
         at = pl.ds(pl.multiple_of(b * block_len, block_len), block_len)
         return partner(read.at[at], read_far.at[at], 3 + b)
 
-    def attend(b, carry):
+    def attend_block(b):
         at = pl.ds(pl.multiple_of(b * block_len, block_len), block_len)
         memory = jnp.concatenate(
-            [final[tab[slot_base + b * per_block + i]] for i in range(per_block)], axis=0
+            [final[tab[2, slot_base + b * per_block + i]] for i in range(per_block)], axis=0
         )
         for h in range(heads):
             cut = slice(h * head_dim, (h + 1) * head_dim)
+            scale = scale_ref[h] * (1.0 / math.sqrt(head_dim))
             scores = lax.dot_general(
                 query[at, cut], memory[:, cut], (((1,), (1,)), ((), ())), preferred_element_type=F32
             )
-            scores = scores * scale_ref[h]
+            scores = scores * scale
             top = jnp.exp(scores - jnp.max(scores, axis=-1, keepdims=True))
             weights = (top * (1.0 / jnp.sum(top, axis=-1, keepdims=True))).astype(BF16)
             read[at, cut] = jnp.dot(
                 weights, memory[:, width + h * head_dim : width + (h + 1) * head_dim], preferred_element_type=F32
             ).astype(BF16)
-        read_swap(b).start()
+
+    unroll = math.gcd(blocks, 4)
+
+    def attend(i, carry):
+        for k in range(unroll):
+            attend_block(i * unroll + k)
+        for k in range(unroll):
+            read_swap(i * unroll + k).start()
         return carry
 
-    lax.fori_loop(0, blocks, attend, 0)
+    with jax.named_scope("attend"):
+        lax.fori_loop(0, blocks // unroll, attend, 0)
 
     def finish(b, carry):
         at = pl.ds(pl.multiple_of(b * block_len, block_len), block_len)
@@ -530,7 +641,8 @@
             out_ref[at, cols] = (branch[at, cols] + gate[at, cols] * terms).astype(BF16)
         return carry
 
-    lax.fori_loop(0, blocks, finish, 0)
+    with jax.named_scope("finish"):
+        lax.fori_loop(0, blocks, finish, 0)
 
     for way in range(2):
         for i, (_, _, need) in enumerate(cuts):
@@ -543,7 +655,7 @@
             spread_copy(rel, q).wait_send()
 
 
-def mixer(planes, caps, most, block_len, collective_id, operands):
+def mixer(planes, most, block_len, per_block, caps, collective_id, *operands):
     tab, scale, gain, mix, kv, hidden, w_pool, w_query, w_gate, w_branch, w_out = operands
     holders = lax.axis_size("st")
     side = holders // planes
@@ -560,7 +672,7 @@
     dma = pltpu.SemaphoreType.DMA
     flops = 2 * tokens * (model * (pool_width + width + half) + 2 * (pool_width + width) * half)
     return pl.pallas_call(
-        functools.partial(mixer_kernel, planes, caps, most, block_len),
+        functools.partial(mixer_kernel, planes, caps, most, block_len, per_block),
         out_shape=jax.ShapeDtypeStruct((tokens, half), BF16),
         in_specs=[SMEM, SMEM, VMEM, VMEM] + [ANY] * 7,
         out_specs=VMEM,
@@ -625,16 +737,19 @@
     pass_dev = store.shape[0]
     tokens, model = hidden.shape
     most = max(1, 2 * reads // holders)
-    head_dim = w_query.shape[1] // sharpness.shape[0]
-
-    all_ids, own_kv = project(passage_ids.reshape(-1), store, store_gain, w_key, w_value)
+
     one = min(pass_dev, side * most)
     full = tuple(min(pass_dev, k * one) for k in range(1, planes))
-    short = tuple(min(f, (11 * one) // 16 + (k > 0) * pass_dev // 6 + (k > 1) * pass_dev // 12) for k, f in enumerate(full))
-    fits, tab = plan(all_ids[:, 0, :reads], planes, pass_dev, most, short)
+    variants = []
+    for sixteenths in (9, 10, 11):
+        first = one * sixteenths // 16
+        lengths = (first, first + pass_dev // 6, first + pass_dev // 4)[: planes - 1]
+        variants.append(tuple(map(min, lengths, full)))
+    variants = (*variants, full)
+    tab, own_kv = project(planes, most, variants, passage_ids, store, store_gain, w_key, w_value)
     operands = (
         tab,
-        sharpness / math.sqrt(head_dim),
+        sharpness,
         norm_gain.reshape(1, model),
         pool_mix,
         own_kv,
@@ -645,13 +760,9 @@
         w_branch,
         w_out,
     )
-    run = functools.partial(mixer, planes)
-    block_len = tokens // blocks
-    return lax.cond(
-        fits,
-        lambda *ops: run(short, most, block_len, 1, ops),
-        lambda *ops: run(full, most, block_len, 2, ops),
-        *operands,
+    run = functools.partial(mixer, planes, most, tokens // blocks, per_block)
+    return lax.switch(
+        tab[3, 0], [functools.partial(run, caps, i + 1) for i, caps in enumerate(variants)], *operands
     )
 
 

time: 106 us -> 85.6 us (0.81)
  Pallas kernels: 86.8 us -> 79.3 us
  other arithmetic: 6.64 us -> 0 us
  between operations: 3.93 us -> 0.7 us
  local copies, waits for them, and re-layouts: 6.96 us -> 4.95 us
    pallas_call x1, Pallas kernels: 74.7 us -> 67.4 us  [mixer(): pl.pallas_call(functools.partial(mixer_kernel, planes, caps, most, block_...]
    reduce_and x6 -> x0, other arithmetic: 3.93 us -> none  [plan(): fits.append(jnp.all(count <= room[:, None]))]
    reduce_sum x7 -> x0, other arithmetic: 1.58 us -> none  [the longest x2 0.57 us: plan(): count = jnp.sum((reach >= d).astype(i32), axis=2)]
    unnamed x24 -> x8, local copies, waits for them, and re-layouts: 4.45 us -> 4.44 us
where the time goes in v2:
time: 85.6 us; the launch traced here: 85.2 us
  Pallas kernels  79.3 us (93%)
  local copies, waits for them, and re-layouts  4.95 us (6%)
    pallas_call x1, Pallas kernels, mixer(): pl.pallas_call(functools.partial(mixer_kernel, planes, caps, most, block_...  67.4 us
    pallas_call x1, Pallas kernels, project(): pl.pallas_call(functools.partial(project_kernel, holders, planes, pieces,...  11.8 us
    unnamed x8, local copies, waits for them, and re-layouts  4.44 us

profile of v2, /device:TPU:13, one launch (start us, length us, event | category | flops | bytes accessed | tf_op | source)
XLA Modules:
  0.0 85.2 jit_solution(1469055328552804599)
XLA Ops:
  0.0 1.3 %copy.19.ids_ref = s32[8,4]{1,0:T(8,128)} copy(s32[8,4]{0,1:T(4,128)} %param.22) | data formatting | bytes 256 | tf_op args[4]
  1.3 0.0 copy-start
  1.4 0.0 copy-start.1
  1.4 0.0 copy-start.2
  1.4 11.8 %shard_map.140 = (s32[24,128]{1,0:T(8,128)S(1)}, bf16[24,64,512]{2,1,0:T(8,128)(2,1)}) custom-call(s32[8,4]{1,0:T(8,128)} %copy.19.ids_ref, bf16[1536,2048]{1,0:T(8,128)(2,1)} %bitcast.4, f32[1,2048]{1,0:T(1,128)} %bitcast.5, bf16[2048,256]{1,0:T(8,128)(2,1)} %wk_ref.1, bf16[2048,256]{1,0:T(8,128)(2,1)} %wv_ref.1), custom_call_target="tpu_custom_call" | custom-call | flops 3221225472 | bytes 6291456 | tf_op jit(solution)/shard_map/pallas_call | solution.py:251
  13.2 0.5 slice.3
  14.4 0.0 copy-done
  14.4 0.0 copy-done.1
  14.4 0.0 copy-done.2
  14.4 67.7 %conditional.1 = (bf16[1024,1024]{1,0:T(8,128)(2,1)}) conditional(s32[]{:T(128)} %bitcast.2, (s32[24,128]{1,0:T(8,128)S(1)}, f32[2]{0:T(128)S(1)}, f32[1,2048]{1,0:T(1,128)S(1)}, bf16[2,256,256]{2,1,0:T(8,128)(2,1)S(1)}, bf16[24,64,512]{2,1,0:T(8,128)(2,1)}, /*index=5*/bf16[1024,2048]{1,0:T(8,128)(2,1)}, ...), branch_computations={%region_0.0_spmd, %region_1.0_spmd, %region_2.0_spmd, %region_3.0_... | conditional | flops 10737418240 | bytes 33554440 | solution.py:764
  14.4 67.4 %branch_0_fun.1 = bf16[1024,1024]{1,0:T(8,128)(2,1)} custom-call(s32[24,128]{1,0:T(8,128)S(1)} %get-tuple-element.96.tab, f32[2]{0:T(128)S(1)} %get-tuple-element.98.scale_ref, f32[1,2048]{1,0:T(1,128)S(1)} %get-tuple-element.100.gain_ref, bf16[2,256,256]{2,1,0:T(8,128)(2,1)S(1)} %get-tuple-element.101.mix_ref, ...), custom_call_target="tpu_custom_call" | custom-call | flops 10737418240 | bytes 33554432 | tf_op jit(solution)/shard_map/cond/branch_0_fun/pallas_call | solution.py:674
  82.1 3.1 %copy.25 = bf16[1024,1024]{1,0:T(8,128)(2,1)} copy(bf16[1024,1024]{1,0:T(8,128)(2,1)} %get-tuple-element.146) | data formatting | bytes 4194304
Async XLA Ops:
  1.3 13.0 %copy-start = (bf16[2,256,256]{2,1,0:T(8,128)(2,1)S(1)}, bf16[2,256,256]{2,1,0:T(8,128)(2,1)}, u32[]{:S(2)}) copy-start(bf16[2,256,256]{2,1,0:T(8,128)(2,1)} %param.24) | copy-start | bytes 786436
  1.4 13.0 %copy-start.1 = (f32[2048]{0:T(1024)S(1)}, f32[2048]{0:T(1024)}, u32[]{:S(2)}) copy-start(f32[2048]{0:T(1024)} %param.19) | copy-start | bytes 24580
  1.4 13.0 %copy-start.2 = (f32[2]{0:T(128)S(1)}, f32[2]{0:T(128)}, u32[]{:S(2)}) copy-start(f32[2]{0:T(128)} %param.29) | copy-start | bytes 28

commit v3 on v2

--- a/solution.py
+++ b/solution.py
@@ -52,6 +52,8 @@
     plane_at = whole(holder_at, side)
     far_up = jnp.zeros((pass_dev, holders), F32)
     far_down = jnp.zeros((pass_dev, holders), F32)
+    near_up = jnp.zeros((pass_dev, holders), F32)
+    near_down = jnp.zeros((pass_dev, holders), F32)
     for p in range(planes):
         hits = jnp.zeros((pass_dev, holders), F32)
         for row in requests(p):
@@ -63,12 +65,17 @@
         ahead = jnp.where(hits > 0.5, p - plane_at, 0.0)
         far_up = jnp.maximum(far_up, ahead)
         far_down = jnp.maximum(far_down, -ahead)
-
-    longest = [jnp.zeros((1, holders), F32) for _ in range(planes - 1)]
+        near_up = jnp.where(ahead == 1.0, 1.0, near_up)
+        near_down = jnp.where(ahead == -1.0, 1.0, near_down)
+
+    longest = [jnp.zeros((1, holders), F32) for _ in range(planes - 2)]
+    for reach, edge in ((near_up, 0), (near_down, planes - 1)):
+        count = jnp.sum(reach, axis=0, keepdims=True)
+        longest[0] = jnp.maximum(longest[0], jnp.where(plane_at == edge, count, 0.0))
     for reach, left in ((far_up, planes - 1 - plane_at), (far_down, plane_at)):
         for d in range(1, planes):
             count = jnp.sum(jnp.where(reach >= d, 1.0, 0.0), axis=0, keepdims=True)
-            for k in range(planes - 1):
+            for k in range(planes - 2):
                 longest[k] = jnp.maximum(longest[k], jnp.where(left - d == k, count, 0.0))
     longest = [jnp.max(x, axis=1, keepdims=True) for x in longest]
     variant = jnp.zeros((1, 1), F32)
@@ -94,11 +101,16 @@
     number = sub_of(pass_dev)
     orders = [
         jnp.sum(jnp.where(place_in(reach, z) == lane_of(pass_dev), number, 0.0), axis=0, keepdims=True)
-        for reach in (far_up, far_down)
+        for reach in (far_up, far_down, jnp.where(z == 0, near_up, near_down))
     ]
     where_at = []
     for q in range(planes):
-        place = place_in(jnp.where(q < z, far_up, far_down), jnp.int32(q))
+        reach = jnp.where(q < z, far_up, far_down)
+        if q == 0:
+            reach = jnp.where(z == 1, near_up, reach)
+        if q == planes - 1:
+            reach = jnp.where(z == planes - 2, near_down, reach)
+        place = place_in(reach, jnp.int32(q))
         where_at.append(jnp.where(q == z, sub_of(pass_dev, 1), place))
 
     square_sub = sub_of(lanes)
@@ -124,7 +136,7 @@
             column = jnp.sum(jnp.where(segment == t, values, 0.0), axis=1, keepdims=True)
             picks = jnp.where(lane_of(planes * most) == r * per + t, column, picks)
         slots = jnp.where(lax.div(c, per) == r, (of_side * planes + of_plane) * most + rank, slots)
-    for i, row in enumerate((*orders, slots, variant + jnp.zeros((1, lanes), F32))):
+    for i, row in enumerate((*orders[:2], slots, variant + jnp.zeros((1, lanes), F32), orders[2])):
         tab_ref[i : i + 1, :] = row.astype(jnp.int32)
     tab_ref[8 : 8 + planes * most, :] = picks.astype(jnp.int32)
 
@@ -146,11 +158,13 @@
     ids_ref,
     store_ref,
     gain_ref,
-    wk_ref,
-    wv_ref,
+    wk_hbm,
+    wv_hbm,
     tab_ref,
     kv_ref,
     rows,
+    wk_ref,
+    wv_ref,
     mine_ids,
     all_ref,
     load_sem,
@@ -163,15 +177,22 @@
     width = wk_ref.shape[1]
     pass_dev, length, _ = kv_ref.shape
     passages = piece // length
-    blocks, per_block = ids_ref.shape
+    per_block, blocks = ids_ref.shape
     reads = blocks * per_block
+    weights = [
+        pltpu.make_async_copy(src, dst, load_sem.at[pieces + i])
+        for i, (src, dst) in enumerate(((wk_hbm, wk_ref), (wv_hbm, wv_ref)))
+    ]
 
     def load(i):
         return pltpu.make_async_copy(
             store_ref.at[pl.ds(i * piece, piece)], rows.at[pl.ds(i * piece, piece)], load_sem.at[i]
         )
 
-    for i in range(pieces):
+    load(0).start()
+    for copy in weights:
+        copy.start()
+    for i in range(1, pieces):
         load(i).start()
 
     barrier = pltpu.get_barrier_semaphore()
@@ -185,15 +206,15 @@
 
     lax.fori_loop(1, holders, greet, 0)
 
-    lane = lax.broadcasted_iota(jnp.int32, (blocks, 128), 1)
-    lane = lane - reads * jnp.floor((lane.astype(F32) + 0.5) * (1.0 / reads)).astype(jnp.int32)
-    block = jnp.floor((lane.astype(F32) + 0.5) * (1.0 / per_block)).astype(jnp.int32)
+    lane = lax.broadcasted_iota(jnp.int32, (per_block, 128), 1).astype(F32)
+    lane = lane - reads * jnp.floor((lane + 0.5) * (1.0 / reads))
+    block = jnp.floor((lane + 0.5) * (1.0 / per_block))
     inner = lane - block * per_block
-    spread_ids = jnp.zeros((blocks, 128), F32)
-    for k in range(per_block):
-        spread_ids = jnp.where(inner == k, ids_ref[:, k : k + 1].astype(F32), spread_ids)
-    at_block = lax.broadcasted_iota(jnp.int32, (blocks, 128), 0) == block
-    row = jnp.sum(jnp.where(at_block, spread_ids, 0.0), axis=0, keepdims=True)
+    spread_ids = jnp.zeros((per_block, 128), F32)
+    for k in range(blocks):
+        spread_ids = jnp.where(block == k, ids_ref[:, k : k + 1].astype(F32), spread_ids)
+    at_inner = lax.broadcasted_iota(jnp.int32, (per_block, 128), 0).astype(F32) == inner
+    row = jnp.sum(jnp.where(at_inner, spread_ids, 0.0), axis=0, keepdims=True)
     mine_ids[...] = jnp.broadcast_to(row, mine_ids.shape).astype(jnp.int32)
     all_ref[me] = jnp.broadcast_to(row, mine_ids.shape).astype(jnp.int32)
 
@@ -208,7 +229,9 @@
             )
         return carry
 
-    first = pieces // 2
+    first = 1
+    for copy in weights:
+        copy.wait()
     with jax.named_scope("kv0"):
         lax.fori_loop(0, first, project, 0)
     with jax.named_scope("greet_all"):
@@ -218,8 +241,8 @@
         return pltpu.make_async_remote_copy(
             src_ref=mine_ids,
             dst_ref=all_ref.at[me],
-            send_sem=send_sem.at[step],
-            recv_sem=recv_sem.at[step],
+            send_sem=send_sem.at[0],
+            recv_sem=recv_sem.at[0],
             device_id=(other(step), core),
             device_id_type=MESH,
         )
@@ -232,12 +255,16 @@
     with jax.named_scope("kv1"):
         lax.fori_loop(first, pieces, project, 0)
 
-    def finish(step, carry):
-        ids_copy(step).wait()
-        return carry
-
+    every = all_ref.at[pl.ds(0, holders - 1)]
     with jax.named_scope("ids"):
-        lax.fori_loop(1, holders, finish, 0)
+        pltpu.make_async_remote_copy(
+            src_ref=every,
+            dst_ref=every,
+            send_sem=send_sem.at[0],
+            recv_sem=recv_sem.at[0],
+            device_id=(other(1), core),
+            device_id_type=MESH,
+        ).wait()
     with jax.named_scope("tables"):
         plan_tables(holders, planes, reads, pass_dev, most, variants, all_ref, tab_ref)
 
@@ -254,21 +281,23 @@
             jax.ShapeDtypeStruct((table_rows, 128), jnp.int32),
             jax.ShapeDtypeStruct((pass_dev, length, 2 * width), BF16),
         ),
-        in_specs=[VMEM, ANY, VMEM, VMEM, VMEM],
+        in_specs=[VMEM, ANY, VMEM, ANY, ANY],
         out_specs=(VMEM, VMEM),
         scratch_shapes=[
             pltpu.VMEM((pass_dev * length, model), BF16),
+            pltpu.VMEM(w_key.shape, BF16),
+            pltpu.VMEM(w_value.shape, BF16),
             pltpu.VMEM((8, 128), jnp.int32),
             pltpu.VMEM((holders, 8, 128), jnp.int32),
-            pltpu.SemaphoreType.DMA((pieces,)),
-            pltpu.SemaphoreType.DMA((holders,)),
-            pltpu.SemaphoreType.DMA((holders,)),
+            pltpu.SemaphoreType.DMA((pieces + 2,)),
+            pltpu.SemaphoreType.DMA((1,)),
+            pltpu.SemaphoreType.DMA((1,)),
         ],
         compiler_params=pltpu.CompilerParams(collective_id=0, has_side_effects=True, vmem_limit_bytes=LIMIT),
         cost_estimate=pl.CostEstimate(
             flops=4 * pass_dev * length * model * width, bytes_accessed=store.size * 2, transcendentals=0
         ),
-    )(ids, store.reshape(pass_dev * length, model), store_gain.reshape(1, model), w_key, w_value)
+    )(ids.T, store.reshape(pass_dev * length, model), store_gain.reshape(1, model), w_key, w_value)
 
 
 def chunks_of(caps):
@@ -319,14 +348,15 @@
 ):
     reach = planes - 1
     lists = [rest[w * reach : (w + 1) * reach] for w in range(2)]
-    picked, final, load_sem, z_send, z_recv, in_send, in_recv, core_send, core_recv = rest[2 * reach :]
+    near_own, near_up, near_down, picked, final, out_rows, load_sem, out_sem, near_send, near_recv, z_send, z_recv, in_send, in_recv, core_send, core_recv = rest[2 * reach :]
     holders = lax.axis_size("st")
     side = holders // planes
     me = lax.axis_index("st")
     core = lax.axis_index("tp")
     z, c = lax.div(me, side), lax.rem(me, side)
     tokens, model = normed.shape
-    half = out_ref.shape[1]
+    half = out_rows.shape[1]
+    near = (near_up, near_down)
     cuts = chunks_of(caps)
     beyond = (planes - 1 - z, z)
     behind = (z, planes - 1 - z)
@@ -405,7 +435,27 @@
             device_id_type=MESH,
         ).wait_recv()
 
-    def forward(d, i):
+    def near_hop(way):
+        return pltpu.make_async_remote_copy(
+            src_ref=near_own,
+            dst_ref=near[way],
+            send_sem=near_send.at[0],
+            recv_sem=near_recv.at[way],
+            device_id=(me + step_to[way], core),
+            device_id_type=MESH,
+        )
+
+    def near_arrive(way):
+        pltpu.make_async_remote_copy(
+            src_ref=near[way],
+            dst_ref=near[way],
+            send_sem=near_send.at[0],
+            recv_sem=near_recv.at[way],
+            device_id=(me, 1 - core),
+            device_id_type=MESH,
+        ).wait_recv()
+
+    def forward(d, i, here):
         need = cuts[i][2]
         if need > reach - d:
             return
@@ -415,14 +465,14 @@
                 arrive(way, d, i)
                 hop(way, d, i).start()
 
-            pl.when((behind[way] >= d) & (beyond[way] >= need))(go)
-
-    def keep(d):
+            pl.when(here(way) & (behind[way] >= d) & (beyond[way] >= need))(go)
+
+    def keep(d, here):
         for i, (_, _, need) in enumerate(cuts):
             if need > reach - d + 1:
                 continue
             for way in range(2):
-                pl.when((behind[way] >= d) & (beyond[way] + 1 == need))(lambda way=way, i=i: arrive(way, d, i))
+                pl.when(here(way) & (behind[way] >= d) & (beyond[way] + 1 == need))(lambda way=way, i=i: arrive(way, d, i))
 
 
     def spread_copy(rel, q):
@@ -446,16 +496,29 @@
         for j in range(most):
             final[(c * planes + q) * most + j] = src[tab[8 + q * most + j, c]]
 
-    def spread_from(d):
+    def spread_from(d, here):
         for way in range(2):
             q = z - d if way == 0 else z + d
-            pl.when(behind[way] >= d)(lambda way=way, q=q: spread(lists[way][d - 1], q))
+            pl.when(here(way) & (behind[way] >= d))(lambda way=way, q=q: spread(lists[way][d - 1], q))
+
+    def spread_near():
+        for way in range(2):
+
+            def go(way=way):
+                near_arrive(way)
+                spread(near[way], z - 1 if way == 0 else z + 1)
+
+            pl.when((behind[way] == 1) & (beyond[way] >= 1))(go)
 
     with jax.named_scope("first_sends"):
         loads[0].wait()
         for way in range(2):
             for s in range(caps[-1]):
                 own_lists[way, s] = kv[tab[way, s]]
+        for s in range(caps[0]):
+            near_own[s] = kv[tab[4, s]]
+        for way in range(2):
+            pl.when(behind[way] == 0)(lambda way=way: near_hop(way).start())
         for i, (_, _, need) in enumerate(cuts):
             for way in range(2):
                 pl.when(beyond[way] >= need)(lambda way=way, i=i: hop(way, 0, i).start())
@@ -537,10 +600,17 @@
             )
         return carry
 
-    def forward_all(d, which):
-        for i in which:
-            if i < len(cuts):
-                forward(d, i)
+    def at_edge(way):
+        return beyond[way] == 0
+
+    def inside(way):
+        return beyond[way] >= 1
+
+    def from_edge(way):
+        return behind[way] == 1
+
+    def from_inside(way):
+        return behind[way] >= 2
 
     with jax.named_scope("norm"):
         loads[1].wait()
@@ -551,13 +621,19 @@
         pool_in[:halo, :] = jnp.zeros((halo, pool_in.shape[1]), BF16)
         project_rows(0, pieces)
     with jax.named_scope("pool"):
-        forward_all(1, [0])
         lax.fori_loop(0, pieces, pool_rows, 0)
         pool_swap.start()
+    with jax.named_scope("step0"):
+        forward(1, 0, from_inside)
     with jax.named_scope("gate"):
         loads[5].wait()
         gate_rows(0, pieces // 2)
-        forward_all(1, [1])
+    with jax.named_scope("step1"):
+        forward(1, 1, from_inside)
+        keep(1, at_edge)
+        spread_from(1, at_edge)
+        spread_near()
+    with jax.named_scope("gate"):
         gate_rows(pieces // 2, pieces)
     with jax.named_scope("branch"):
         loads[4].wait()
@@ -566,16 +642,24 @@
             copy.wait()
         pool_swap.wait()
         lax.fori_loop(0, pieces, branch_rows, 0)
-    with jax.named_scope("spread1"):
-        forward_all(1, range(2, len(cuts)))
-        keep(1)
-        spread_from(1)
+    with jax.named_scope("step2"):
+        for i in range(2, len(cuts)):
+            forward(1, i, from_inside)
+        keep(1, inside)
+        spread_from(1, lambda way: inside(way) & from_inside(way))
+        forward(1, 0, from_edge)
     for d in range(2, planes):
-        with jax.named_scope(f"spread{d}"):
-            if d < planes - 1:
-                forward_all(d, range(len(cuts)))
-            keep(d)
-            spread_from(d)
+        with jax.named_scope(f"step{d + 1}"):
+            forward(d, 0, inside)
+            keep(d, at_edge)
+            spread_from(d, at_edge)
+            if d == 2:
+                for i in range(1, len(cuts)):
+                    forward(1, i, from_edge)
+            for i in range(1, len(cuts)):
+                forward(d, i, inside)
+            keep(d, inside)
+            spread_from(d, inside)
 
     with jax.named_scope("arrivals"):
         for rel in range(1, side):
@@ -632,13 +716,18 @@
     with jax.named_scope("attend"):
         lax.fori_loop(0, blocks // unroll, attend, 0)
 
+    def out_copy(b):
+        at = pl.ds(pl.multiple_of(b * block_len, block_len), block_len)
+        return pltpu.make_async_copy(out_rows.at[at], out_ref.at[at], out_sem.at[b])
+
     def finish(b, carry):
         at = pl.ds(pl.multiple_of(b * block_len, block_len), block_len)
         read_swap(b).wait()
         for j in range(2):
             cols = slice(j * half // 2, (j + 1) * half // 2)
             terms = two_terms(read[at, :], w_out[:, cols], read_far[at, :], w_out_far[:, cols])
-            out_ref[at, cols] = (branch[at, cols] + gate[at, cols] * terms).astype(BF16)
+            out_rows[at, cols] = (branch[at, cols] + gate[at, cols] * terms).astype(BF16)
+        out_copy(b).start()
         return carry
 
     with jax.named_scope("finish"):
@@ -653,6 +742,10 @@
     for rel in range(1, side):
         for q in range(planes):
             spread_copy(rel, q).wait_send()
+    for way in range(2):
+        pl.when(behind[way] == 0)(lambda way=way: near_hop(way).wait_send())
+    for b in range(blocks):
+        out_copy(b).wait()
 
 
 def mixer(planes, most, block_len, per_block, caps, collective_id, *operands):
@@ -675,7 +768,7 @@
         functools.partial(mixer_kernel, planes, caps, most, block_len, per_block),
         out_shape=jax.ShapeDtypeStruct((tokens, half), BF16),
         in_specs=[SMEM, SMEM, VMEM, VMEM] + [ANY] * 7,
-        out_specs=VMEM,
+        out_specs=ANY,
         scratch_shapes=[
             v(kv.shape, BF16),
             v(hidden.shape, BF16),
@@ -695,10 +788,15 @@
             v((tokens, width), BF16),
             v((tokens, width), BF16),
             v((2, caps[-1], *slot), BF16),
-            *[v((caps[reach - d], *slot), BF16) for _ in range(2) for d in range(1, planes)],
+            *[v((caps[min(reach - d, reach - 2)], *slot), BF16) for _ in range(2) for d in range(1, planes)],
+            *[v((caps[0], *slot), BF16) for _ in range(3)],
             v((side - 1, planes * most, *slot), BF16),
             v((holders * most, *slot), BF16),
+            v((tokens, half), BF16),
             dma((7,)),
+            dma((blocks,)),
+            dma((1,)),
+            dma((2,)),
             dma((2, reach, nch)),
             dma((2, reach, nch)),
             dma((side - 1, planes)),
@@ -739,11 +837,11 @@
     most = max(1, 2 * reads // holders)
 
     one = min(pass_dev, side * most)
-    full = tuple(min(pass_dev, k * one) for k in range(1, planes))
+    full = tuple(min(pass_dev, k * one) for k in range(1, planes - 1))
     variants = []
     for sixteenths in (9, 10, 11):
         first = one * sixteenths // 16
-        lengths = (first, first + pass_dev // 6, first + pass_dev // 4)[: planes - 1]
+        lengths = (first, first + pass_dev // 6)
         variants.append(tuple(map(min, lengths, full)))
     variants = (*variants, full)
     tab, own_kv = project(planes, most, variants, passage_ids, store, store_gain, w_key, w_value)

time: 85.6 us -> 77.8 us (0.909)
  Pallas kernels: 79.3 us -> 72.9 us
  local copies, waits for them, and re-layouts: 4.95 us -> 3.61 us
    pallas_call x1, Pallas kernels: 67.4 us -> 63 us  [mixer(): pl.pallas_call(functools.partial(mixer_kernel, planes, caps, most, block_...]
    pallas_call x1, Pallas kernels: 11.8 us -> 9.91 us  [project(): pl.pallas_call(functools.partial(project_kernel, holders, planes, pieces,...]
    unnamed x8 -> x7, local copies, waits for them, and re-layouts: 4.44 us -> 3.09 us
where the time goes in v3:
time: 77.8 us; the launch traced here: 77.5 us
  Pallas kernels  72.9 us (94%)
  local copies, waits for them, and re-layouts  3.61 us (5%)
    pallas_call x1, Pallas kernels, mixer(): pl.pallas_call(functools.partial(mixer_kernel, planes, caps, most, block_...  63 us
    pallas_call x1, Pallas kernels, project(): pl.pallas_call(functools.partial(project_kernel, holders, planes, pieces,...  9.91 us
    unnamed x7, local copies, waits for them, and re-layouts  3.09 us

profile of v3, /device:TPU:13, one launch (start us, length us, event | category | flops | bytes accessed | tf_op | source)
XLA Modules:
  0.0 77.5 jit_solution(30812520755535756)
XLA Ops:
  0.0 0.0 copy-start
  0.0 0.0 copy-start.1
  0.0 0.0 copy-start.2
  0.0 9.9 %shard_map.140 = (s32[24,128]{1,0:T(8,128)S(1)}, bf16[24,64,512]{2,1,0:T(8,128)(2,1)}) custom-call(s32[4,8]{1,0:T(4,128)} %bitcast.11, bf16[1536,2048]{1,0:T(8,128)(2,1)} %bitcast.5, f32[1,2048]{1,0:T(1,128)} %bitcast.6, bf16[2048,256]{1,0:T(8,128)(2,1)} %wk_hbm.1, bf16[2048,256]{1,0:T(8,128)(2,1)} %wv_hbm.1), custom_call_target="tpu_custom_call" | custom-call | flops 3221225472 | bytes 6291456 | tf_op jit(solution)/shard_map/pallas_call | solution.py:278
  9.9 0.5 slice.3
  11.1 0.0 copy-done
  11.1 0.0 copy-done.1
  11.1 0.0 copy-done.2
  11.1 63.2 %conditional.1 = (bf16[1024,1024]{1,0:T(8,128)(2,1)}) conditional(s32[]{:T(128)} %bitcast.3, (s32[24,128]{1,0:T(8,128)S(1)}, f32[2]{0:T(128)S(1)}, f32[1,2048]{1,0:T(1,128)S(1)}, bf16[2,256,256]{2,1,0:T(8,128)(2,1)S(1)}, bf16[24,64,512]{2,1,0:T(8,128)(2,1)}, /*index=5*/bf16[1024,2048]{1,0:T(8,128)(2,1)}, ...), branch_computations={%region_0.0_spmd, %region_1.0_spmd, %region_2.0_spmd, %region_3.0_... | conditional | flops 10737418240 | bytes 33554440 | solution.py:862
  11.1 63.0 %branch_0_fun.1 = bf16[1024,1024]{1,0:T(8,128)(2,1)} custom-call(s32[24,128]{1,0:T(8,128)S(1)} %get-tuple-element.96.tab, f32[2]{0:T(128)S(1)} %get-tuple-element.98.scale_ref, f32[1,2048]{1,0:T(1,128)S(1)} %get-tuple-element.100.gain_ref, bf16[2,256,256]{2,1,0:T(8,128)(2,1)S(1)} %get-tuple-element.101.mix_ref, ...), custom_call_target="tpu_custom_call" | custom-call | flops 10737418240 | bytes 33554432 | tf_op jit(solution)/shard_map/cond/branch_0_fun/pallas_call | solution.py:767
  74.4 3.1 %copy.24 = bf16[1024,1024]{1,0:T(8,128)(2,1)} copy(bf16[1024,1024]{1,0:T(8,128)(2,1)} %get-tuple-element.146) | data formatting | bytes 4194304
Async XLA Ops:
  0.0 11.1 %copy-start = (bf16[2,256,256]{2,1,0:T(8,128)(2,1)S(1)}, bf16[2,256,256]{2,1,0:T(8,128)(2,1)}, u32[]{:S(2)}) copy-start(bf16[2,256,256]{2,1,0:T(8,128)(2,1)} %param.24) | copy-start | bytes 786436
  0.0 11.1 %copy-start.1 = (f32[2048]{0:T(1024)S(1)}, f32[2048]{0:T(1024)}, u32[]{:S(2)}) copy-start(f32[2048]{0:T(1024)} %param.19) | copy-start | bytes 24580
  0.0 11.1 %copy-start.2 = (f32[2]{0:T(128)S(1)}, f32[2]{0:T(128)}, u32[]{:S(2)}) copy-start(f32[2]{0:T(128)} %param.29) | copy-start | bytes 28

commit v4 on v3

--- a/solution.py
+++ b/solution.py
@@ -14,7 +14,6 @@
 ANY = pl.BlockSpec(memory_space=pl.ANY)
 VMEM = pl.BlockSpec(memory_space=pltpu.VMEM)
 SMEM = pl.BlockSpec(memory_space=pltpu.SMEM)
-LIMIT = 66_000_000
 
 
 def planes_of(mesh):
@@ -161,10 +160,13 @@
     wk_hbm,
     wv_hbm,
     tab_ref,
+    kv_out,
     kv_ref,
     rows,
     wk_ref,
     wv_ref,
+    even,
+    odd,
     mine_ids,
     all_ref,
     load_sem,
@@ -218,22 +220,22 @@
     mine_ids[...] = jnp.broadcast_to(row, mine_ids.shape).astype(jnp.int32)
     all_ref[me] = jnp.broadcast_to(row, mine_ids.shape).astype(jnp.int32)
 
-    def project(i, carry):
+    def norm(i, ref):
         load(i).wait()
         start = pl.multiple_of(i * piece, piece)
-        normed = rms_rows(rows[pl.ds(start, piece), :].astype(F32), gain_ref[...]).astype(BF16)
+        ref[...] = rms_rows(rows[pl.ds(start, piece), :].astype(F32), gain_ref[...]).astype(BF16)
+
+    def project(i, ref):
         for half, w_ref in enumerate((wk_ref, wv_ref)):
-            part = jnp.dot(normed, w_ref[...], preferred_element_type=F32).astype(BF16)
+            part = jnp.dot(ref[...], w_ref[...], preferred_element_type=F32).astype(BF16)
             kv_ref[pl.ds(i * passages, passages), :, half * width : (half + 1) * width] = part.reshape(
                 passages, length, width
             )
-        return carry
-
-    first = 1
-    for copy in weights:
-        copy.wait()
+
     with jax.named_scope("kv0"):
-        lax.fori_loop(0, first, project, 0)
+        norm(0, even)
+        for copy in weights:
+            copy.wait()
     with jax.named_scope("greet_all"):
         pl.semaphore_wait(barrier, holders - 1)
 
@@ -252,8 +254,18 @@
         return carry
 
     lax.fori_loop(1, holders, send, 0)
+
+    def leave(i):
+        at = pl.ds(i * passages, passages)
+        return pltpu.make_async_copy(kv_ref.at[at], kv_out.at[at], load_sem.at[pieces + 2 + i])
+
     with jax.named_scope("kv1"):
-        lax.fori_loop(first, pieces, project, 0)
+        for i in range(pieces):
+            if i + 1 < pieces:
+                norm(i + 1, (even, odd)[(i + 1) % 2])
+            project(i, (even, odd)[i % 2])
+            if i:
+                leave(i - 1).start()
 
     every = all_ref.at[pl.ds(0, holders - 1)]
     with jax.named_scope("ids"):
@@ -266,7 +278,10 @@
             device_id_type=MESH,
         ).wait()
     with jax.named_scope("tables"):
+        leave(pieces - 1).start()
         plan_tables(holders, planes, reads, pass_dev, most, variants, all_ref, tab_ref)
+    for i in range(pieces):
+        leave(i).wait()
 
 
 def project(planes, most, variants, ids, store, store_gain, w_key, w_value):
@@ -282,18 +297,21 @@
             jax.ShapeDtypeStruct((pass_dev, length, 2 * width), BF16),
         ),
         in_specs=[VMEM, ANY, VMEM, ANY, ANY],
-        out_specs=(VMEM, VMEM),
+        out_specs=(VMEM, ANY),
         scratch_shapes=[
+            pltpu.VMEM((pass_dev, length, 2 * width), BF16),
             pltpu.VMEM((pass_dev * length, model), BF16),
             pltpu.VMEM(w_key.shape, BF16),
             pltpu.VMEM(w_value.shape, BF16),
+            pltpu.VMEM((pass_dev * length // pieces, model), BF16),
+            pltpu.VMEM((pass_dev * length // pieces, model), BF16),
             pltpu.VMEM((8, 128), jnp.int32),
             pltpu.VMEM((holders, 8, 128), jnp.int32),
-            pltpu.SemaphoreType.DMA((pieces + 2,)),
+            pltpu.SemaphoreType.DMA((2 * pieces + 2,)),
             pltpu.SemaphoreType.DMA((1,)),
             pltpu.SemaphoreType.DMA((1,)),
         ],
-        compiler_params=pltpu.CompilerParams(collective_id=0, has_side_effects=True, vmem_limit_bytes=LIMIT),
+        compiler_params=pltpu.CompilerParams(collective_id=0, has_side_effects=True, vmem_limit_bytes=66_000_000),
         cost_estimate=pl.CostEstimate(
             flops=4 * pass_dev * length * model * width, bytes_accessed=store.size * 2, transcendentals=0
         ),
@@ -386,14 +404,18 @@
     def greet(device):
         pl.semaphore_signal(barrier, inc=1, device_id=device, device_id_type=MESH)
 
-    plane_mates = [z * side + lax.rem(c + rel, side) for rel in range(1, side)]
-    for mate in plane_mates:
-        greet((mate, core))
+    def mate_of(k):
+        mate = c
+        for b in range(k.bit_length()):
+            if k >> b & 1:
+                mate = mate + (1 << b) * (1 - 2 * lax.rem(lax.div(c, 1 << b), 2))
+        return mate
+
+    for k in range(1, side):
+        greet((z * side + mate_of(k), core))
     greet((me, 1 - core))
     for way in range(2):
         pl.when(beyond[way] >= 1)(lambda way=way: greet((me + step_to[way], core)))
-    with jax.named_scope("greet"):
-        pl.semaphore_wait(barrier, side + (z + reach - 1) // reach + (beyond[0] + reach - 1) // reach)
 
     def partner(src, dst, i):
         return pltpu.make_async_remote_copy(
@@ -476,7 +498,7 @@
 
 
     def spread_copy(rel, q):
-        mate = z * side + lax.rem(c + rel, side)
+        mate = z * side + mate_of(rel)
         return pltpu.make_async_remote_copy(
             src_ref=picked.at[rel - 1, pl.ds(q * most, most)],
             dst_ref=final.at[pl.ds((c * planes + q) * most, most)],
@@ -486,15 +508,21 @@
             device_id_type=MESH,
         )
 
+    mates = list(range(side - 1, 0, -1))
+
+    def pick(src, q, k):
+        for j in range(most):
+            slot = src[tab[8 + q * most + j, mate_of(k) if k else c]]
+            if k:
+                picked[k - 1, q * most + j] = slot
+            else:
+                final[(c * planes + q) * most + j] = slot
+
     def spread(src, q):
-        for rel in range(1, side):
-            mate = lax.rem(c + rel, side)
-            for j in range(most):
-                picked[rel - 1, q * most + j] = src[tab[8 + q * most + j, mate]]
-        for rel in range(1, side):
-            spread_copy(rel, q).start()
-        for j in range(most):
-            final[(c * planes + q) * most + j] = src[tab[8 + q * most + j, c]]
+        for n, k in enumerate((*mates, 0)):
+            pick(src, q, k)
+            if n:
+                spread_copy(mates[n - 1], q).start()
 
     def spread_from(d, here):
         for way in range(2):
@@ -510,19 +538,25 @@
 
             pl.when((behind[way] == 1) & (beyond[way] >= 1))(go)
 
-    with jax.named_scope("first_sends"):
+    with jax.named_scope("build"):
         loads[0].wait()
         for way in range(2):
             for s in range(caps[-1]):
                 own_lists[way, s] = kv[tab[way, s]]
         for s in range(caps[0]):
             near_own[s] = kv[tab[4, s]]
+        for k in range(side):
+            pick(kv, z, k)
+    with jax.named_scope("greet"):
+        pl.semaphore_wait(barrier, side + (z + reach - 1) // reach + (beyond[0] + reach - 1) // reach)
+    with jax.named_scope("first_sends"):
         for way in range(2):
             pl.when(behind[way] == 0)(lambda way=way: near_hop(way).start())
         for i, (_, _, need) in enumerate(cuts):
             for way in range(2):
                 pl.when(beyond[way] >= need)(lambda way=way, i=i: hop(way, 0, i).start())
-        spread(kv, z)
+        for k in mates:
+            spread_copy(k, z).start()
         for copy in weight_swaps:
             copy.start()
 
@@ -663,7 +697,7 @@
 
     with jax.named_scope("arrivals"):
         for rel in range(1, side):
-            source = lax.rem(c + side - rel, side)
+            source = mate_of(rel)
             for q in range(planes):
                 at = pl.ds((source * planes + q) * most, most)
                 pltpu.make_async_remote_copy(
@@ -716,22 +750,25 @@
     with jax.named_scope("attend"):
         lax.fori_loop(0, blocks // unroll, attend, 0)
 
-    def out_copy(b):
-        at = pl.ds(pl.multiple_of(b * block_len, block_len), block_len)
-        return pltpu.make_async_copy(out_rows.at[at], out_ref.at[at], out_sem.at[b])
-
-    def finish(b, carry):
-        at = pl.ds(pl.multiple_of(b * block_len, block_len), block_len)
-        read_swap(b).wait()
+    joint = math.gcd(blocks, 2)
+
+    def out_copy(i):
+        at = pl.ds(pl.multiple_of(i * joint * block_len, block_len), joint * block_len)
+        return pltpu.make_async_copy(out_rows.at[at], out_ref.at[at], out_sem.at[i])
+
+    def finish(i, carry):
+        at = pl.ds(pl.multiple_of(i * joint * block_len, block_len), joint * block_len)
+        for k in range(joint):
+            read_swap(i * joint + k).wait()
         for j in range(2):
             cols = slice(j * half // 2, (j + 1) * half // 2)
             terms = two_terms(read[at, :], w_out[:, cols], read_far[at, :], w_out_far[:, cols])
             out_rows[at, cols] = (branch[at, cols] + gate[at, cols] * terms).astype(BF16)
-        out_copy(b).start()
+        out_copy(i).start()
         return carry
 
     with jax.named_scope("finish"):
-        lax.fori_loop(0, blocks, finish, 0)
+        lax.fori_loop(0, blocks // joint, finish, 0)
 
     for way in range(2):
         for i, (_, _, need) in enumerate(cuts):
@@ -744,8 +781,8 @@
             spread_copy(rel, q).wait_send()
     for way in range(2):
         pl.when(behind[way] == 0)(lambda way=way: near_hop(way).wait_send())
-    for b in range(blocks):
-        out_copy(b).wait()
+    for i in range(blocks // joint):
+        out_copy(i).wait()
 
 
 def mixer(planes, most, block_len, per_block, caps, collective_id, *operands):
@@ -805,7 +842,7 @@
             dma((3 + blocks,)),
         ],
         compiler_params=pltpu.CompilerParams(
-            collective_id=collective_id, has_side_effects=True, vmem_limit_bytes=LIMIT
+            collective_id=collective_id, has_side_effects=True, vmem_limit_bytes=55 * 2**20
         ),
         cost_estimate=pl.CostEstimate(flops=flops, bytes_accessed=32 * 2**20, transcendentals=0),
     )(*operands)

time: 77.8 us -> 74.2 us (0.954)
  Pallas kernels: 72.9 us -> 70.9 us
  local copies, waits for them, and re-layouts: 3.61 us -> 1.85 us
    pallas_call x1, Pallas kernels: 63 us -> 60.9 us  [mixer(): pl.pallas_call(functools.partial(mixer_kernel, planes, caps, most, block_...]
    unnamed x7, local copies, waits for them, and re-layouts: 3.09 us -> 1.33 us
where the time goes in v4:
time: 74.2 us; the launch traced here: 73.9 us
  Pallas kernels  70.9 us (96%)
  local copies, waits for them, and re-layouts  1.85 us (2%)
    pallas_call x1, Pallas kernels, mixer(): pl.pallas_call(functools.partial(mixer_kernel, planes, caps, most, block_...  60.9 us
    pallas_call x1, Pallas kernels, project(): pl.pallas_call(functools.partial(project_kernel, holders, planes, pieces,...  10 us

profile of v4, /device:TPU:13, one launch (start us, length us, event | category | flops | bytes accessed | tf_op | source)
XLA Modules:
  0.0 73.9 jit_solution(6597865670118541188)
XLA Ops:
  0.0 0.0 copy-start
  0.0 0.0 copy-start.1
  0.0 0.0 copy-start.2
  0.0 10.0 %shard_map.140 = (s32[24,128]{1,0:T(8,128)S(1)}, bf16[24,64,512]{2,1,0:T(8,128)(2,1)}) custom-call(s32[4,8]{1,0:T(4,128)} %bitcast.11, bf16[1536,2048]{1,0:T(8,128)(2,1)} %bitcast.5, f32[1,2048]{1,0:T(1,128)} %bitcast.6, bf16[2048,256]{1,0:T(8,128)(2,1)} %wk_hbm.1, bf16[2048,256]{1,0:T(8,128)(2,1)} %wv_hbm.1), custom_call_target="tpu_custom_call" | custom-call | flops 3221225472 | bytes 6291456 | tf_op jit(solution)/shard_map/pallas_call | solution.py:293
  10.0 0.5 slice.3
  11.2 0.0 copy-done
  11.2 0.0 copy-done.1
  11.2 0.0 copy-done.2
  11.2 61.3 %conditional.1 = (bf16[1024,1024]{1,0:T(8,128)(2,1)S(1)}) conditional(s32[]{:T(128)} %bitcast.3, (s32[24,128]{1,0:T(8,128)S(1)}, f32[2]{0:T(128)S(1)}, f32[1,2048]{1,0:T(1,128)S(1)}, bf16[2,256,256]{2,1,0:T(8,128)(2,1)S(1)}, bf16[24,64,512]{2,1,0:T(8,128)(2,1)}, /*index=5*/bf16[1024,2048]{1,0:T(8,128)(2,1)}, ...), branch_computations={%region_0.0_spmd, %region_1.0_spmd, %region_2.0_spmd, %region_3.0_... | conditional | flops 10737418240 | bytes 33554440 | solution.py:899
  11.3 60.9 %branch_0_fun.1 = bf16[1024,1024]{1,0:T(8,128)(2,1)S(1)} custom-call(s32[24,128]{1,0:T(8,128)S(1)} %get-tuple-element.96.tab, f32[2]{0:T(128)S(1)} %get-tuple-element.98.scale_ref, f32[1,2048]{1,0:T(1,128)S(1)} %get-tuple-element.100.gain_ref, bf16[2,256,256]{2,1,0:T(8,128)(2,1)S(1)} %get-tuple-element.101.mix_ref, ...), custom_call_target="tpu_custom_call" | custom-call | flops 10737418240 | bytes 33554432 | tf_op jit(solution)/shard_map/cond/branch_0_fun/pallas_call | solution.py:804
  72.6 1.3 %copy.24 = bf16[1024,1024]{1,0:T(8,128)(2,1)} copy(bf16[1024,1024]{1,0:T(8,128)(2,1)S(1)} %get-tuple-element.146) | data formatting | bytes 4194304
Async XLA Ops:
  0.0 11.2 %copy-start = (bf16[2,256,256]{2,1,0:T(8,128)(2,1)S(1)}, bf16[2,256,256]{2,1,0:T(8,128)(2,1)}, u32[]{:S(2)}) copy-start(bf16[2,256,256]{2,1,0:T(8,128)(2,1)} %param.24) | copy-start | bytes 786436
  0.0 11.2 %copy-start.1 = (f32[2048]{0:T(1024)S(1)}, f32[2048]{0:T(1024)}, u32[]{:S(2)}) copy-start(f32[2048]{0:T(1024)} %param.19) | copy-start | bytes 24580
  0.0 11.2 %copy-start.2 = (f32[2]{0:T(128)S(1)}, f32[2]{0:T(128)}, u32[]{:S(2)}) copy-start(f32[2]{0:T(128)} %param.29) | copy-start | bytes 28

commit v5 on v4

--- a/solution.py
+++ b/solution.py
@@ -13,6 +13,7 @@
 BF16 = jnp.bfloat16
 ANY = pl.BlockSpec(memory_space=pl.ANY)
 VMEM = pl.BlockSpec(memory_space=pltpu.VMEM)
+PIN = pl.BlockSpec(memory_space=pltpu.HBM)
 SMEM = pl.BlockSpec(memory_space=pltpu.SMEM)
 
 
@@ -160,7 +161,6 @@
     wk_hbm,
     wv_hbm,
     tab_ref,
-    kv_out,
     kv_ref,
     rows,
     wk_ref,
@@ -255,17 +255,11 @@
 
     lax.fori_loop(1, holders, send, 0)
 
-    def leave(i):
-        at = pl.ds(i * passages, passages)
-        return pltpu.make_async_copy(kv_ref.at[at], kv_out.at[at], load_sem.at[pieces + 2 + i])
-
     with jax.named_scope("kv1"):
         for i in range(pieces):
             if i + 1 < pieces:
                 norm(i + 1, (even, odd)[(i + 1) % 2])
             project(i, (even, odd)[i % 2])
-            if i:
-                leave(i - 1).start()
 
     every = all_ref.at[pl.ds(0, holders - 1)]
     with jax.named_scope("ids"):
@@ -278,10 +272,7 @@
             device_id_type=MESH,
         ).wait()
     with jax.named_scope("tables"):
-        leave(pieces - 1).start()
         plan_tables(holders, planes, reads, pass_dev, most, variants, all_ref, tab_ref)
-    for i in range(pieces):
-        leave(i).wait()
 
 
 def project(planes, most, variants, ids, store, store_gain, w_key, w_value):
@@ -294,12 +285,11 @@
         functools.partial(project_kernel, holders, planes, pieces, most, variants),
         out_shape=(
             jax.ShapeDtypeStruct((table_rows, 128), jnp.int32),
-            jax.ShapeDtypeStruct((pass_dev, length, 2 * width), BF16),
+            pltpu.VMEM((pass_dev, length, 2 * width), BF16),
         ),
-        in_specs=[VMEM, ANY, VMEM, ANY, ANY],
-        out_specs=(VMEM, ANY),
+        in_specs=[VMEM, PIN, VMEM, PIN, PIN],
+        out_specs=(VMEM, VMEM),
         scratch_shapes=[
-            pltpu.VMEM((pass_dev, length, 2 * width), BF16),
             pltpu.VMEM((pass_dev * length, model), BF16),
             pltpu.VMEM(w_key.shape, BF16),
             pltpu.VMEM(w_value.shape, BF16),
@@ -311,7 +301,7 @@
             pltpu.SemaphoreType.DMA((1,)),
             pltpu.SemaphoreType.DMA((1,)),
         ],
-        compiler_params=pltpu.CompilerParams(collective_id=0, has_side_effects=True, vmem_limit_bytes=66_000_000),
+        compiler_params=pltpu.CompilerParams(collective_id=0, has_side_effects=True, vmem_limit_bytes=65_250_000),
         cost_estimate=pl.CostEstimate(
             flops=4 * pass_dev * length * model * width, bytes_accessed=store.size * 2, transcendentals=0
         ),
@@ -336,7 +326,7 @@
     scale_ref,
     gain_ref,
     mix_ref,
-    kv_hbm,
+    kv,
     hidden_hbm,
     w_pool_hbm,
     w_query_hbm,
@@ -344,7 +334,6 @@
     w_branch_hbm,
     w_out_hbm,
     out_ref,
-    kv,
     normed,
     w_pool,
     w_query,
@@ -386,7 +375,6 @@
         pltpu.make_async_copy(src, dst, load_sem.at[i])
         for i, (src, dst) in enumerate(
             (
-                (kv_hbm, kv),
                 (hidden_hbm, normed),
                 (w_pool_hbm, w_pool),
                 (w_query_hbm, w_query),
@@ -539,7 +527,6 @@
             pl.when((behind[way] == 1) & (beyond[way] >= 1))(go)
 
     with jax.named_scope("build"):
-        loads[0].wait()
         for way in range(2):
             for s in range(caps[-1]):
                 own_lists[way, s] = kv[tab[way, s]]
@@ -647,11 +634,11 @@
         return behind[way] >= 2
 
     with jax.named_scope("norm"):
-        loads[1].wait()
+        loads[0].wait()
         norm(0, tokens)
     with jax.named_scope("project"):
+        loads[1].wait()
         loads[2].wait()
-        loads[3].wait()
         pool_in[:halo, :] = jnp.zeros((halo, pool_in.shape[1]), BF16)
         project_rows(0, pieces)
     with jax.named_scope("pool"):
@@ -660,7 +647,7 @@
     with jax.named_scope("step0"):
         forward(1, 0, from_inside)
     with jax.named_scope("gate"):
-        loads[5].wait()
+        loads[4].wait()
         gate_rows(0, pieces // 2)
     with jax.named_scope("step1"):
         forward(1, 1, from_inside)
@@ -670,8 +657,8 @@
     with jax.named_scope("gate"):
         gate_rows(pieces // 2, pieces)
     with jax.named_scope("branch"):
-        loads[4].wait()
-        loads[6].wait()
+        loads[3].wait()
+        loads[5].wait()
         for copy in weight_swaps:
             copy.wait()
         pool_swap.wait()
@@ -804,10 +791,9 @@
     return pl.pallas_call(
         functools.partial(mixer_kernel, planes, caps, most, block_len, per_block),
         out_shape=jax.ShapeDtypeStruct((tokens, half), BF16),
-        in_specs=[SMEM, SMEM, VMEM, VMEM] + [ANY] * 7,
+        in_specs=[SMEM, SMEM, VMEM, VMEM, VMEM] + [PIN] * 6,
         out_specs=ANY,
         scratch_shapes=[
-            v(kv.shape, BF16),
             v(hidden.shape, BF16),
             v(w_pool.shape, BF16),
             v(w_query.shape, BF16),
@@ -830,7 +816,7 @@
             v((side - 1, planes * most, *slot), BF16),
             v((holders * most, *slot), BF16),
             v((tokens, half), BF16),
-            dma((7,)),
+            dma((6,)),
             dma((blocks,)),
             dma((1,)),
             dma((2,)),

time: 74.2 us -> 74 us (level)
  no operation moved by 1% of the time
where the time goes in v5:
time: 74 us; the launch traced here: 73.8 us
  Pallas kernels  70.8 us (96%)
  local copies, waits for them, and re-layouts  1.84 us (2%)
    pallas_call x1, Pallas kernels, mixer(): pl.pallas_call(functools.partial(mixer_kernel, planes, caps, most, block_...  61.2 us
    pallas_call x1, Pallas kernels, project(): pl.pallas_call(functools.partial(project_kernel, holders, planes, pieces,...  9.64 us

profile of v5, /device:TPU:13, one launch (start us, length us, event | category | flops | bytes accessed | tf_op | source)
XLA Modules:
  0.0 73.8 jit_solution(299743274457620185)
XLA Ops:
  0.0 0.0 copy-start
  0.0 0.0 copy-start.1
  0.0 9.6 %shard_map.140 = (s32[24,128]{1,0:T(8,128)S(1)}, bf16[24,64,512]{2,1,0:T(8,128)(2,1)S(1)}) custom-call(s32[4,8]{1,0:T(4,128)} %bitcast.11, bf16[1536,2048]{1,0:T(8,128)(2,1)} %bitcast.5, f32[1,2048]{1,0:T(1,128)} %bitcast.6, bf16[2048,256]{1,0:T(8,128)(2,1)} %wk_hbm.1, bf16[2048,256]{1,0:T(8,128)(2,1)} %wv_hbm.1), custom_call_target="tpu_custom_call" | custom-call | flops 3221225472 | bytes 6291456 | tf_op jit(solution)/shard_map/pallas_call | solution.py:284
  9.6 0.5 slice.3
  10.8 0.0 copy-done
  10.8 0.0 copy-done.1
  10.8 61.6 %conditional.1 = (bf16[1024,1024]{1,0:T(8,128)(2,1)S(1)}) conditional(s32[]{:T(128)} %bitcast.3, (s32[24,128]{1,0:T(8,128)S(1)}, f32[2]{0:T(128)S(1)}, f32[1,2048]{1,0:T(1,128)S(1)}, bf16[2,256,256]{2,1,0:T(8,128)(2,1)}, bf16[24,64,512]{2,1,0:T(8,128)(2,1)S(1)}, /*index=5*/bf16[1024,2048]{1,0:T(8,128)(2,1)}, ...), branch_computations={%region_0.0_spmd, %region_1.0_spmd, %region_2.0_spmd, %region_3.0_... | conditional | flops 10737418240 | bytes 33554440 | solution.py:885
  10.9 61.2 %branch_0_fun.1 = bf16[1024,1024]{1,0:T(8,128)(2,1)S(1)} custom-call(s32[24,128]{1,0:T(8,128)S(1)} %get-tuple-element.96.tab, f32[2]{0:T(128)S(1)} %get-tuple-element.98.scale_ref, f32[1,2048]{1,0:T(1,128)S(1)} %get-tuple-element.100.gain_ref, bf16[2,256,256]{2,1,0:T(8,128)(2,1)} %get-tuple-element.101.mix_ref, ...), custom_call_target="tpu_custom_call" | custom-call | flops 10737418240 | bytes 33554432 | tf_op jit(solution)/shard_map/cond/branch_0_fun/pallas_call | solution.py:791
  72.4 1.3 %copy.24 = bf16[1024,1024]{1,0:T(8,128)(2,1)} copy(bf16[1024,1024]{1,0:T(8,128)(2,1)S(1)} %get-tuple-element.146) | data formatting | bytes 4194304
Async XLA Ops:
  0.0 10.8 %copy-start = (f32[2048]{0:T(1024)S(1)}, f32[2048]{0:T(1024)}, u32[]{:S(2)}) copy-start(f32[2048]{0:T(1024)} %param.19) | copy-start | bytes 24580
  0.0 10.8 %copy-start.1 = (f32[2]{0:T(128)S(1)}, f32[2]{0:T(128)}, u32[]{:S(2)}) copy-start(f32[2]{0:T(128)} %param.29) | copy-start | bytes 28
